TPU v7x, 512 devices: a whole 4x4x16 slice. The times are simulated.
512 devices in a mesh: fs: 128 (over z, x, core), tp: 4 (over y).
Axes of the slice: x: 4, y: 4, z: 16, core: 2. Of those that a mesh axis runs over, the one named last changes fastest.
Arguments:
- block_input: bfloat16 [131072, 2048], P(('fs', 'tp')), may hold values from -6 to 6
- gate_cotangent: bfloat16 [131072, 2048], P('fs', 'tp'), may hold values from -0.016479492 to 0.016479492
- gated_state: bfloat16 [131072, 2048], P('fs', 'tp'), may hold values from -6 to 6
- mixer_cotangent: bfloat16 [131072, 2048], P(('fs', 'tp')), may hold values from -0.016479492 to 0.016479492
- gate_basis: bfloat16 [2048, 512], P('fs'), may hold values from -0.125 to 0.125
- out_basis: bfloat16 [2048, 512], P('fs'), may hold values from -0.125 to 0.125
- gate_master: float32 [2048, 2048], P('fs', 'tp'), may hold values from -0.6 to 0.6
- out_master: float32 [2048, 2048], P('tp', 'fs'), may hold values from -0.6 to 0.6
- gate_first: float32 [512, 2048], P('fs', 'tp'), may hold values from -3 to 3
- gate_second: float32 [512, 2048], P('fs', 'tp'), may hold values from 0.01 to 8.1, as said below
- out_first: float32 [512, 2048], P('fs', 'tp'), may hold values from -3 to 3
- out_second: float32 [512, 2048], P('fs', 'tp'), may hold values from 0.01 to 8.1, as said below
Outputs:
- gate_master_new: float32 [2048, 2048], P('fs', 'tp')
- out_master_new: float32 [2048, 2048], P('tp', 'fs')
- gate_copy: bfloat16 [2048, 2048], P(None, 'tp')
- out_copy: bfloat16 [2048, 2048], P('tp')
- gate_first_new: float32 [512, 2048], P('fs', 'tp')
- gate_second_new: float32 [512, 2048], P('fs', 'tp')
- out_first_new: float32 [512, 2048], P('fs', 'tp')
- out_second_new: float32 [512, 2048], P('fs', 'tp')
Inputs may be any that keep to these rules, and one draw needn't show every extreme that they name: `gate_second`: positive. `out_second`: positive.
All inputs are finite; a program needn't handle non-finite values.
Results may differ from a plain program's by a relative error of at most 0.0038.
Values may be sent and summed in bfloat16 or wider, within the bound.
A program may use at most 64 MiB of HBM per device.

v0:
```python
import jax
import jax.numpy as jnp
from jax import lax
from jax.sharding import Mesh
from jax.sharding import PartitionSpec as P

FS = ("fs_0", "fs_1", "fs_2")
FS_TP = ("fs_0", "fs_1", "fs_2", "tp")


def copy_for_each(x, axis):
    peers = lax.axis_size(axis)
    return lax.all_to_all(jnp.broadcast_to(x[None], (peers, *x.shape)), axis, 0, 0, tiled=True)


def joined_along(tiles, dim):
    shape = list(tiles.shape[1:])
    shape[dim] *= tiles.shape[0]
    return jnp.moveaxis(tiles, 0, dim).reshape(shape)


def gather_axes(x, axes, dim):
    far, near = axes
    tiles = copy_for_each(copy_for_each(x, far), near)
    return joined_along(tiles.swapaxes(0, 1).reshape(-1, *x.shape), dim)


def side_by_side(arrays, axis, dim, along):
    widths = [a.shape[along] for a in arrays]
    both = jnp.concatenate(arrays, axis=along)
    filled = gather_axes(both, axis, dim)
    return tuple(jnp.split(filled, [sum(widths[:k]) for k in range(1, len(widths))], axis=along))


def in_one_piece(arrays, axis, dim, along):
    ends, at = ([], 0)
    for a in arrays[:-1]:
        at += a.shape[along]
        ends.append(at)
    both = jnp.concatenate(arrays, axis=along)
    return tuple(jnp.split(lax.all_gather(both, axis, axis=dim, tiled=True), ends, axis=along))


def cut_along(x, dim, peers):
    shape = x.shape
    tiles = x.reshape(*shape[:dim], peers, shape[dim] // peers, *shape[dim + 1 :])
    return jnp.moveaxis(tiles, dim, 0)


def summed_on_arrival(x, axis, dim):
    tiles = cut_along(x, dim, lax.axis_size(axis))
    arrived = lax.all_to_all(tiles, axis, split_axis=0, concat_axis=0, tiled=True)
    return arrived.astype(jnp.float32).sum(axis=0)


def summed_rows(x, axes, dim):
    far, near = axes
    tiles = cut_along(x, dim, lax.axis_size(far))
    nearer = summed_on_arrival(tiles, near, dim + 1)
    arrived = lax.all_to_all(
        nearer.astype(jnp.bfloat16), far, split_axis=0, concat_axis=0, tiled=True
    )
    return arrived.astype(jnp.float32).sum(axis=0)


def of_everyone(x, axis):
    return copy_for_each(x, axis).sum(axis=0)


def add_pieces(left_first, left_second, pieces):
    return (
        jnp.dot(left_first, pieces[0], preferred_element_type=jnp.float32),
        jnp.dot(left_second, pieces[1], preferred_element_type=jnp.float32),
    )


def on_device(
    block_input,
    gate_cotangent,
    gated_state,
    mixer_cotangent,
    gate_basis,
    out_basis,
    gate_master,
    out_master,
    gate_first,
    gate_second,
    out_first,
    out_second,
):
    low_rank = gate_basis.shape[1]
    local_cols = gate_first.shape[1]
    tp_count = lax.axis_size("tp")
    part_in, part_cot = add_pieces(
        block_input,
        mixer_cotangent,
        side_by_side((gate_basis, out_basis), (("fs_0", "fs_1"), "fs_2"), 0, 1),
    )
    proj_in, proj_cot = in_one_piece(
        (part_in.astype(jnp.bfloat16), part_cot.astype(jnp.bfloat16)), "tp", 0, 1
    )
    contract = (((0,), (0,)), ((), ()))
    gate_term = lax.dot_general(
        proj_in, gate_cotangent, contract, preferred_element_type=jnp.float32
    )
    out_term = lax.dot_general(proj_cot, gated_state, contract, preferred_element_type=jnp.float32)
    summed = summed_rows(
        jnp.concatenate([gate_term, out_term], axis=1).astype(jnp.bfloat16),
        (("fs_0", "fs_1"), "fs_2"),
        0,
    )
    first_old = jnp.concatenate([gate_first, out_first], axis=1)
    second_old = jnp.concatenate([gate_second, out_second], axis=1)
    first_new = 0.9 * first_old + 0.1 * summed
    second_new = 0.95 * second_old + 0.05 * summed * summed
    raw_step = first_new / jnp.sqrt(second_new)
    own_squares = jnp.sum(raw_step * raw_step)
    full_step, row_squares = (
        gather_axes(raw_step, (("fs_0", "fs_1"), "fs_2"), 0),
        gather_axes(own_squares.reshape(1), (("fs_0", "fs_1"), "fs_2"), 0),
    )
    squares = of_everyone(jnp.sum(row_squares), "tp")
    norm_scale = lax.rsqrt(squares / (2.0 * low_rank * local_cols * tp_count) + 1e-06)
    gate_scaled = full_step[:, :local_cols] * norm_scale
    out_scaled = full_step[:, local_cols:] * norm_scale
    gate_update = jnp.dot(
        gate_basis.astype(jnp.float32), gate_scaled, precision=lax.Precision.HIGHEST
    )
    out_update = lax.dot_general(
        out_scaled,
        out_basis.astype(jnp.float32),
        (((0,), (1,)), ((), ())),
        precision=lax.Precision.HIGHEST,
    )
    gate_master_new = gate_master - 0.25 * gate_update
    out_master_new = out_master - 0.25 * out_update
    gate_copy, out_copy = (
        gather_axes(gate_master_new.astype(jnp.bfloat16), (("fs_0", "fs_1"), "fs_2"), 0),
        gather_axes(out_master_new.astype(jnp.bfloat16), (("fs_0", "fs_1"), "fs_2"), 1),
    )
    return (
        gate_master_new,
        out_master_new,
        gate_copy,
        out_copy,
        first_new[:, :local_cols],
        second_new[:, :local_cols],
        first_new[:, local_cols:],
        second_new[:, local_cols:],
    )


def solution(mesh):
    finer = Mesh(mesh.devices.reshape(16, 4, 2, mesh.shape["tp"]), ("fs_0", "fs_1", "fs_2", "tp"))
    in_specs = (
        P(FS_TP, None),
        P(FS, "tp"),
        P(FS, "tp"),
        P(FS_TP, None),
        P(FS, None),
        P(FS, None),
        P(FS, "tp"),
        P("tp", FS),
        P(FS, "tp"),
        P(FS, "tp"),
        P(FS, "tp"),
        P(FS, "tp"),
    )
    out_specs = (
        P(FS, "tp"),
        P("tp", FS),
        P(None, "tp"),
        P("tp", None),
        P(FS, "tp"),
        P(FS, "tp"),
        P(FS, "tp"),
        P(FS, "tp"),
    )
    return jax.shard_map(
        on_device, mesh=finer, in_specs=in_specs, out_specs=out_specs, check_vma=False
    )
```

profile of v0, /device:TPU:1, one launch (start us, length us, event | category | flops | bytes accessed | tf_op | source)
XLA Modules:
  0.0 493.0 jit_solution(8937257196890186143)
XLA Ops:
  8.3 113.9 %all_to_all.67 = bf16[64,16,1024]{2,1,0:T(8,128)(2,1)S(1)} all-to-all(bf16[64,16,1024]{2,1,0:T(8,128)(2,1)S(1)} %broadcast_in_dim.24), channel_id=1, replica_groups=mesh['fs_0'=16,'fs_1'=4,'fs_2'=2,'tp'=4] {'fs_0','fs_1'}, dimensions={0} | all-to-all | bytes 4194304 | tf_op jit(solution)/shard_map/all_to_all | solution.py:13
  122.8 12.9 %all_to_all.68 = bf16[2,64,16,1024]{3,2,1,0:T(8,128)(2,1)S(1)} all-to-all(bf16[2,64,16,1024]{3,2,1,0:T(8,128)(2,1)S(1)} %broadcast_in_dim.25), channel_id=1, replica_groups=mesh['fs_0'=16,'fs_1'=4,'fs_2'=2,'tp'=4] {'fs_2'}, dimensions={0} | all-to-all | bytes 8388608 | tf_op jit(solution)/shard_map/all_to_all | solution.py:13
  139.8 31.9 %all-gather.2.cloned.1.call-done = bf16[1024,1024]{0,1:T(8,128)(2,1)} async-done(((bf16[256,1024]{0,1:T(8,128)(2,1)}), bf16[1024,1024]{0,1:T(8,128)(2,1)}) %all-gather.2.cloned.1.call-update) | async-done | bytes 2097168 | tf_op jit(solution)/shard_map/all_gather | solution.py:41
  171.7 1.9 convolution_convert_fusion.1
  173.7 2.2 convolution_convert_fusion
  176.6 6.2 %all_to_all.69 = bf16[2,64,4,1024]{3,2,1,0:T(4,128)(2,1)S(1)} all-to-all(bf16[2,64,4,1024]{3,2,1,0:T(4,128)(2,1)S(1)} %copy_bitcast_fusion), channel_id=1, replica_groups=mesh['fs_0'=16,'fs_1'=4,'fs_2'=2,'tp'=4] {'fs_2'}, dimensions={0} | all-to-all | bytes 2097152 | tf_op jit(solution)/shard_map/all_to_all | solution.py:52
  183.9 46.1 %all_to_all.70 = bf16[64,4,1024]{2,1,0:T(4,128)(2,1)S(1)} all-to-all(bf16[64,4,1024]{2,1,0:T(4,128)(2,1)S(1)} %reduce_sum.48), channel_id=1, replica_groups=mesh['fs_0'=16,'fs_1'=4,'fs_2'=2,'tp'=4] {'fs_0','fs_1'}, dimensions={0} | all-to-all | bytes 1048576 | tf_op jit(solution)/shard_map/all_to_all | solution.py:60
  231.6 20.5 %all_to_all.71 = f32[64,1,1]{2,1,0:T(1,128)S(1)} all-to-all(f32[64,1,1]{2,1,0:T(1,128)S(1)} %broadcast_in_dim.28), channel_id=1, replica_groups=mesh['fs_0'=16,'fs_1'=4,'fs_2'=2,'tp'=4] {'fs_0','fs_1'}, dimensions={0} | all-to-all | bytes 512 | tf_op jit(solution)/shard_map/all_to_all | solution.py:13
  252.6 5.9 %all_to_all.72 = f32[2,64,1]{1,2,0:T(1,128)S(1)} all-to-all(f32[2,64,1]{1,2,0:T(1,128)S(1)} %broadcast_in_dim.30), channel_id=1, replica_groups=mesh['fs_0'=16,'fs_1'=4,'fs_2'=2,'tp'=4] {'fs_2'}, dimensions={0} | all-to-all | bytes 1024 | tf_op jit(solution)/shard_map/all_to_all | solution.py:13
  259.8 7.6 %all_to_all.73 = f32[4,1,1]{2,1,0:T(1,128)S(1)} all-to-all(f32[4,1,1]{2,1,0:T(1,128)S(1)} %broadcast_in_dim.31), channel_id=1, replica_groups=mesh['fs_0'=16,'fs_1'=4,'fs_2'=2,'tp'=4] {'tp'}, dimensions={0} | all-to-all | bytes 32 | tf_op jit(solution)/shard_map/all_to_all | solution.py:13
  268.6 4.7 all-to-all-start.4
  274.6 50.1 %all-to-all-done.4 = f32[64,4,1024]{2,1,0:T(4,128)S(1)} async-done(((f32[64,4,1024]{2,1,0:T(4,128)}), f32[64,4,1024]{2,1,0:T(4,128)S(1)}, u32[]{:S(2)}, u32[]{:S(2)}) %all-to-all-start.4) | async-done | bytes 1048608 | tf_op jit(solution)/shard_map/all_to_all | solution.py:13
  325.2 10.0 %all_to_all.74 = f32[2,64,4,1024]{3,2,1,0:T(4,128)S(1)} all-to-all(f32[2,64,4,1024]{3,2,1,0:T(4,128)S(1)} %broadcast_in_dim.27), channel_id=1, replica_groups=mesh['fs_0'=16,'fs_1'=4,'fs_2'=2,'tp'=4] {'fs_2'}, dimensions={0} | all-to-all | bytes 4194304 | tf_op jit(solution)/shard_map/all_to_all | solution.py:13
  336.6 2.0 reshape_reshape.12
  340.9 5.8 %all-to-all-start.11 = ((bf16[64,512,16]{1,2,0:T(8,128)(2,1)}), bf16[64,512,16]{1,2,0:T(8,128)(2,1)}, u32[]{:S(2)}, u32[]{:S(2)}) async-start(bf16[64,512,16]{1,2,0:T(8,128)(2,1)} %broadcast_in_dim.34), calls=%async_computation.11 | async-start | bytes 2097152 | tf_op jit(solution)/shard_map/all_to_all | solution.py:13
  347.9 51.3 %all-to-all-done.11 = bf16[64,512,16]{1,2,0:T(8,128)(2,1)} async-done(((bf16[64,512,16]{1,2,0:T(8,128)(2,1)}), bf16[64,512,16]{1,2,0:T(8,128)(2,1)}, u32[]{:S(2)}, u32[]{:S(2)}) %all-to-all-start.11) | async-done | bytes 1048608 | tf_op jit(solution)/shard_map/all_to_all | solution.py:13
  400.3 7.9 %all-to-all-start.9 = ((bf16[64,16,512]{2,1,0:T(8,128)(2,1)}), bf16[64,16,512]{2,1,0:T(8,128)(2,1)S(1)}, u32[]{:S(2)}, u32[]{:S(2)}) async-start(bf16[64,16,512]{2,1,0:T(8,128)(2,1)} %broadcast_in_dim.32), calls=%async_computation.9 | async-start | bytes 2097152 | tf_op jit(solution)/shard_map/all_to_all | solution.py:13
  408.8 50.6 %all-to-all-done.9 = bf16[64,16,512]{2,1,0:T(8,128)(2,1)S(1)} async-done(((bf16[64,16,512]{2,1,0:T(8,128)(2,1)}), bf16[64,16,512]{2,1,0:T(8,128)(2,1)S(1)}, u32[]{:S(2)}, u32[]{:S(2)}) %all-to-all-start.9) | async-done | bytes 1048608 | tf_op jit(solution)/shard_map/all_to_all | solution.py:13
  460.9 10.9 %all_to_all.75 = bf16[2,64,512,16]{2,3,1,0:T(8,128)(2,1)} all-to-all(bf16[2,64,512,16]{2,3,1,0:T(8,128)(2,1)S(1)} %broadcast_in_dim.35), channel_id=1, replica_groups=mesh['fs_0'=16,'fs_1'=4,'fs_2'=2,'tp'=4] {'fs_2'}, dimensions={0} | all-to-all | bytes 4194304 | tf_op jit(solution)/shard_map/all_to_all | solution.py:13
  471.8 1.6 broadcast_in_dim.33
  473.4 4.1 all-to-all-start.10
  477.5 3.1 copy.58
  480.7 3.9 copy.59
  484.6 1.6 copy.57
  (53 shorter events, 21.2 us)
Async XLA Ops:
  7.2 164.5 %copy-start = (bf16[1024,512]{1,0:T(8,128)(2,1)S(1)}, bf16[1024,512]{1,0:T(8,128)(2,1)}, u32[]{:S(2)}) copy-start(bf16[1024,512]{1,0:T(8,128)(2,1)} %param.13) | copy-start | bytes 3145732
  7.2 164.5 %all-gather.2.cloned.1.call-start = ((), (), s32[]{:S(2)}) async-start(), calls=%async_computation.13 | async-start | bytes 2621440 | tf_op jit(solution)/shard_map/all_gather | solution.py:41
  135.7 1.2 copy-start.9
  136.9 1.2 copy-start.10
  182.8 47.4 %copy-start.5 = (f32[4,512]{1,0:T(4,128)S(1)}, f32[4,512]{1,0:T(4,128)}, u32[]{:S(2)}) copy-start(f32[4,512]{1,0:T(4,128)} %param.23) | copy-start | bytes 24580
  182.8 47.4 %copy-start.6 = (f32[4,512]{1,0:T(4,128)S(1)}, f32[4,512]{1,0:T(4,128)}, u32[]{:S(2)}) copy-start(f32[4,512]{1,0:T(4,128)} %param.21) | copy-start | bytes 24580
  182.8 47.4 %copy-start.7 = (f32[4,512]{1,0:T(4,128)S(1)}, f32[4,512]{1,0:T(4,128)}, u32[]{:S(2)}) copy-start(f32[4,512]{1,0:T(4,128)} %param.22) | copy-start | bytes 24580
  182.8 47.5 %copy-start.8 = (f32[4,512]{1,0:T(4,128)S(1)}, f32[4,512]{1,0:T(4,128)}, u32[]{:S(2)}) copy-start(f32[4,512]{1,0:T(4,128)} %param.20) | copy-start | bytes 24580
  268.6 56.0 %all-to-all-start.4 = ((f32[64,4,1024]{2,1,0:T(4,128)}), f32[64,4,1024]{2,1,0:T(4,128)S(1)}, u32[]{:S(2)}, u32[]{:S(2)}) async-start(f32[64,4,1024]{2,1,0:T(4,128)} %broadcast_in_dim.26), calls=%async_computation.4 | async-start | bytes 2097152 | tf_op jit(solution)/shard_map/all_to_all | solution.py:13
  336.6 2.0 copy-start.1
  336.6 2.0 copy-start.3
  338.7 8.1 %copy-start.2 = (bf16[16,512]{1,0:T(8,128)(2,1)S(1)}, bf16[16,512]{1,0:T(8,128)(2,1)}, u32[]{:S(2)}) copy-start(bf16[16,512]{1,0:T(8,128)(2,1)} %param.16) | copy-start | bytes 49156
  338.7 8.1 %copy-start.4 = (f32[16,512]{1,0:T(8,128)S(1)}, f32[16,512]{1,0:T(8,128)}, u32[]{:S(2)}) copy-start(f32[16,512]{1,0:T(8,128)} %param.18) | copy-start | bytes 98308
  340.9 58.3 %all-to-all-start.11 = ((bf16[64,512,16]{1,2,0:T(8,128)(2,1)}), bf16[64,512,16]{1,2,0:T(8,128)(2,1)}, u32[]{:S(2)}, u32[]{:S(2)}) async-start(bf16[64,512,16]{1,2,0:T(8,128)(2,1)} %broadcast_in_dim.34), calls=%async_computation.11 | async-start | bytes 2097152 | tf_op jit(solution)/shard_map/all_to_all | solution.py:13
  400.3 59.2 %all-to-all-start.9 = ((bf16[64,16,512]{2,1,0:T(8,128)(2,1)}), bf16[64,16,512]{2,1,0:T(8,128)(2,1)S(1)}, u32[]{:S(2)}, u32[]{:S(2)}) async-start(bf16[64,16,512]{2,1,0:T(8,128)(2,1)} %broadcast_in_dim.32), calls=%async_computation.9 | async-start | bytes 2097152 | tf_op jit(solution)/shard_map/all_to_all | solution.py:13
  473.4 11.2 %all-to-all-start.10 = ((bf16[2,64,16,512]{3,2,1,0:T(8,128)(2,1)}), bf16[2,64,16,512]{3,2,1,0:T(8,128)(2,1)S(1)}, u32[]{:S(2)}, u32[]{:S(2)}) async-start(bf16[2,64,16,512]{3,2,1,0:T(8,128)(2,1)} %broadcast_in_dim.33), calls=%async_computation.10 | async-start | bytes 4194304 | tf_op jit(solution)/shard_map/all_to_all | solution.py:13
Sparse Core Ops, SparseCore 0:
  139.9 31.7 all-gather.1
where the time goes:
time: 494 us; the launch traced here: 493 us
  blocking collectives  234 us (47%)
  waiting for transfers between devices  184 us (37%)
  local copies, waits for them, and re-layouts  23.8 us (5%)
  starting transfers between devices  22.6 us (5%)
  between operations  15 us (3%)
  matrix products  7.92 us (2%)
  other arithmetic  5.77 us (1%)
    all_to_all x7, blocking collectives, copy_for_each(): lax.all_to_all(jnp.broadcast_to(x[None], (peers, *x.shape)), axis, 0, 0,...  182 us
    all_to_all x4, waiting for transfers between devices, copy_for_each(): lax.all_to_all(jnp.broadcast_to(x[None], (peers, *x.shape)), axis, 0, 0,...  152 us
    all_to_all x1, blocking collectives, summed_rows(): lax.all_to_all(nearer.astype(jnp.bfloat16), far, split_axis=0, concat_axi...  46.1 us
    all_gather x1, waiting for transfers between devices, in_one_piece(): lax.all_gather(both, axis, axis=dim, tiled=True)  31.9 us
    all_to_all x4, starting transfers between devices, copy_for_each(): lax.all_to_all(jnp.broadcast_to(x[None], (peers, *x.shape)), axis, 0, 0,...  22.5 us
  transfers between devices with their start and end apart: 5, of which 4 were waited for; matrix products, arithmetic and copies ran while one was open for 2% of the time, Pallas kernels for 0%

commit v1 on v0

v1 whole, which is shorter than its diff:
```python
import functools

import jax
import jax.numpy as jnp
from jax import lax
from jax.experimental import pallas as pl
from jax.experimental.pallas import tpu as pltpu
from jax.sharding import Mesh
from jax.sharding import PartitionSpec as P

MESH = pl.DeviceIdType.MESH
BF = jnp.bfloat16
F32 = jnp.float32
ZN, XN, YN = 16, 4, 4
FSN = ("z", "x", "core")
FS_TP = ("z", "x", "core", "tp")
NC = 4
ZQ = ZN // NC
OWN = 8
NID = ZN


def block_id(sign, dist):
    return 2 * dist - 1 if sign > 0 else 2 * dist


def remote(src, dst, send, recv, **to):
    return pltpu.make_async_remote_copy(
        src_ref=src, dst_ref=dst, send_sem=send, recv_sem=recv, device_id=to, device_id_type=MESH
    )


def kernel(
    low_rank, inner,
    bi, gc, gs, mc, gb, ob, gmb, omb, gm, om, gf, gsec, of, osec,
    gm_out, om_out, gcopy, ocopy, gf_out, gs_out, of_out, os_out,
    X, C, BB, MB, PT, LB, XR, ZS, ZR, RAW, FS, NM, PM, SQ, GO, OO, GM, OM, GMO, OMO,
    li, ss, sr, ms,
    b_zs, b_zr, b_xs, b_xr, b_os, b_or,
    m_zs, m_zr, m_xs, m_xr, m_os, m_or,
    d_s, d_r,
    y_s, y_r, yo_s, yo_r,
    rx_s, rx_r, rz_s, rz_r,
    az_s, az_r, ax_s, ax_r, ad_s, ad_r,
    pm_s, pm_r, sq_s, sq_r, out_s,
):
    z, x, c, y = (lax.axis_index(a) for a in ("z", "x", "core", "tp"))
    other = 1 - c

    def zat(k):
        return lax.rem(z + k + ZN, ZN)

    def xat(k):
        return lax.rem(x + k + XN, XN)

    def yat(k):
        return lax.rem(y + k + YN, YN)

    own_rows = pl.ds(pl.multiple_of(c * 16, 16), 16)
    dsts = (
        lambda m: BB.at[m, z, x, own_rows],
        lambda m: X.at[c],
        lambda m: C.at[c],
        lambda m: MB.at[m, z, x, own_rows],
        lambda m: FS.at[0, c],
        lambda m: FS.at[1, c],
    )
    gates = (gb, bi, gc, gmb, gf, gsec)
    outs = (ob, mc, gs, omb, of, osec)

    def load(mine):
        for k in range(6):
            pltpu.make_async_copy(mine[k], dsts[k](c), li.at[k]).start()

    def ship(theirs):
        for k in range(6):
            remote(theirs[k], dsts[k](other), ss.at[k], sr.at[k], core=other).start()

    pl.when(c == 0)(lambda: load(gates))
    pl.when(c == 1)(lambda: load(outs))
    pltpu.make_async_copy(gm, GM, ms.at[0]).start()
    pltpu.make_async_copy(om, OM, ms.at[1]).start()

    barrier = pltpu.get_barrier_semaphore()
    for k in (1, -1, 2, -2):
        pl.semaphore_signal(barrier, inc=1, device_id={"z": zat(k)}, device_id_type=MESH)
    for k in (1, -1):
        pl.semaphore_signal(barrier, inc=1, device_id={"x": xat(k)}, device_id_type=MESH)
        pl.semaphore_signal(barrier, inc=1, device_id={"tp": yat(k)}, device_id_type=MESH)
    pl.semaphore_signal(barrier, inc=1, device_id={"core": other}, device_id_type=MESH)
    pl.semaphore_wait(barrier, 9)

    pl.when(c == 0)(lambda: ship(outs))
    pl.when(c == 1)(lambda: ship(gates))

    def arrived(k):
        ref = dsts[k](c)
        pltpu.make_async_copy(gates[k], ref, li.at[k]).wait()
        remote(ref, ref, ss.at[k], sr.at[k], core=other).wait_recv()

    def gather(buf, zs, zr, xs, xr, os, orr):
        def zof(i):
            d = (i + 1) // 2
            odd = lax.rem(i, 2)
            return lax.rem(z + ZN + (1 - 2 * odd) * d, ZN)

        def zsends(s):
            for sign, far in ((1, ZN // 2), (-1, ZN // 2 - 1)):
                src = buf.at[zat(-sign * 2 * s), x]
                for k in (2, 1):
                    if 2 * s + k <= far:
                        i = block_id(sign, 2 * s + k)
                        remote(src, src, zs.at[i], zr.at[i], z=zat(sign * k)).start()

        def zwait(i):
            ref = buf.at[zof(i), x]
            remote(ref, ref, zs.at[i], zr.at[i], z=zat(1)).wait_recv()

        def forward(i):
            ref = buf.at[zof(i), x]
            remote(ref, ref, xs.at[0, i], xr.at[0, i], x=xat(1)).start()
            remote(ref, ref, xs.at[1, i], xr.at[1, i], x=xat(-1)).start()

        def halves(i):
            zz = zof(i)
            return buf.at[zz, xat(-1), pl.ds(0, 16)], buf.at[zz, xat(1), pl.ds(16, 16)]

        def relay(i):
            zz = zof(i)
            left, right = buf.at[zz, xat(-1)], buf.at[zz, xat(1)]
            remote(left, left, xs.at[0, i], xr.at[0, i], x=xat(1)).wait_recv()
            remote(right, right, xs.at[1, i], xr.at[1, i], x=xat(-1)).wait_recv()
            a, b = halves(i)
            remote(a, a, os.at[0, i], orr.at[0, i], x=xat(1)).start()
            remote(b, b, os.at[1, i], orr.at[1, i], x=xat(-1)).start()

        def opposite(i):
            zz = zof(i)
            for h in range(2):
                ref = buf.at[zz, xat(2), pl.ds(16 * h, 16)]
                remote(ref, ref, os.at[h, i], orr.at[h, i], x=xat(1)).wait_recv()

        def drain(i):
            zz = zof(i)
            ref = buf.at[zz, x]
            for h in range(2):
                remote(ref, ref, xs.at[h, i], xr.at[h, i], x=xat(1)).wait_send()
                half = buf.at[zz, x, pl.ds(0, 16)]
                remote(half, half, os.at[h, i], orr.at[h, i], x=xat(1)).wait_send()

        def zdrain(i):
            ref = buf.at[z, x]
            remote(ref, ref, zs.at[i], zr.at[i], z=zat(1)).wait_send()

        def each(f, lo, hi):
            def body(i, _):
                f(i)
                return 0
            lax.fori_loop(lo, hi, body, 0)

        def both(lo, hi):
            for i in range(lo, hi):
                zwait(i)
                forward(i)

        def step0():
            zsends(0)
            forward(0)

        def step(s):
            for i in (4 * s - 1, 4 * s):
                zwait(i)
            zsends(s)
            for i in (4 * s - 3, 4 * s - 2):
                zwait(i)
            each(forward, 4 * s - 3, 4 * s + 1)
            each(relay, max(0, 4 * s - 7), 4 * s - 3)

        def step4():
            both(13, 16)
            each(relay, 9, 13)

        def step5():
            each(relay, 13, 16)

        def step6():
            each(opposite, 0, 16)

        def finish():
            each(zdrain, 1, 16)
            each(drain, 0, 16)

        steps = [step0] + [functools.partial(step, s) for s in (1, 2, 3)] + [step4, step5, step6]
        return steps, finish

    basis_steps, basis_finish = gather(BB.at[c], b_zs, b_zr, b_xs, b_xr, b_os, b_or)
    master_steps, master_finish = gather(MB.at[c], m_zs, m_zr, m_xs, m_xr, m_os, m_or)

    arrived(0)
    for step in basis_steps[:4]:
        step()
    arrived(3)
    master_steps[0]()
    for step in basis_steps[4:]:
        step()

    whole = [
        remote(BB.at[c], BB.at[c], d_s.at[0], d_r.at[0], core=other),
        remote(MB.at[c], MB.at[c], d_s.at[1], d_r.at[1], core=other),
    ]
    whole[0].start()

    arrived(1)
    W = low_rank // NC
    tokens = 512

    def y_copies(u):
        ref = PT.at[y, u]
        return [
            remote(ref, ref, y_s.at[0, u], y_r.at[0, u], tp=yat(1)),
            remote(ref, ref, y_s.at[1, u], y_r.at[1, u], tp=yat(-1)),
        ]

    for u in range(NC):
        basis = BB[c, :, :, :, u * W : (u + 1) * W].reshape(ZN * XN * 32, W)
        proj = jnp.dot(X[...].reshape(tokens, -1), basis, preferred_element_type=F32)
        PT[y, u] = proj.T.astype(BF)
        for copy in y_copies(u):
            copy.start()

    master_steps[1]()
    arrived(2)
    arrived(4)
    arrived(5)

    def y_relays(u):
        left, right = PT.at[yat(-1), u], PT.at[yat(1), u]
        a, b = PT.at[yat(-1), u, pl.ds(0, W // 2)], PT.at[yat(1), u, pl.ds(W // 2, W // 2)]
        return (
            remote(left, left, y_s.at[0, u], y_r.at[0, u], tp=yat(1)),
            remote(right, right, y_s.at[1, u], y_r.at[1, u], tp=yat(-1)),
            remote(a, a, yo_s.at[0, u], yo_r.at[0, u], tp=yat(1)),
            remote(b, b, yo_s.at[1, u], yo_r.at[1, u], tp=yat(-1)),
        )

    def y_stage(u):
        l, r, a, b = y_relays(u)
        l.wait_recv()
        a.start()
        r.wait_recv()
        b.start()

    def rx_copies(u):
        return [
            remote(LB.at[u, xat(d)], XR.at[u, d - 1], rx_s.at[u, d - 1], rx_r.at[u, d - 1], x=xat(d))
            for d in (1, 2, 3)
        ]

    def low_stage(u):
        for h in range(2):
            ref = PT.at[yat(2), u, pl.ds(h * (W // 2), W // 2)]
            remote(ref, ref, yo_s.at[h, u], yo_r.at[h, u], tp=yat(1)).wait_recv()

        def add(k, total):
            rows = pl.ds(pl.multiple_of(k * 256, 256), 256)
            for h in range(2):
                total += jnp.dot(
                    PT[k, u, :, h * 256 : (h + 1) * 256], C[h, rows], preferred_element_type=F32
                )
            return total

        total = lax.fori_loop(0, YN, add, jnp.zeros((W, inner), F32))
        LB[u] = total.reshape(XN, ZQ, OWN, inner).astype(BF)
        for copy in rx_copies(u):
            copy.start()

    def rz_copy(u, q):
        to = q * NC + u
        return remote(ZS.at[u, q], ZR.at[z], rz_s.at[u, q], rz_r.at[z], z=to)

    def rx_stage(u):
        total = LB[u, x].astype(F32)
        for d, copy in enumerate(rx_copies(u)):
            copy.wait_recv()
            total += XR[u, d].astype(F32)
        ZS[u] = total.astype(BF)
        for q in range(ZQ):
            pl.when(z != q * NC + u)(lambda: rz_copy(u, q).start())

    zq = z // NC

    def az_copy(u, d):
        ref = RAW.at[c, u, x, zq]
        return remote(ref, ref, az_s.at[d], az_r.at[u, zq], z=zat(d))

    def pm_copy():
        return remote(NM.at[other], PM, pm_s, pm_r, core=other)

    def rz_stage(u):
        @pl.when(lax.rem(z, NC) == u)
        def _():
            def add(d, total):
                src = zat(d)
                ref = ZR.at[src]
                remote(ref, ref, rz_s.at[u, 0], rz_r.at[src], z=src).wait_recv()
                return total + ZR[src].astype(F32)

            low = lax.fori_loop(1, ZN, add, ZS[u, zq].astype(F32))
            raws = []
            for h in range(2):
                part = low[4 * h : 4 * h + 4]
                first = 0.9 * FS[0, h] + 0.1 * part
                second = 0.95 * FS[1, h] + 0.05 * part * part
                NM[h, 0] = first
                NM[h, 1] = second
                raws.append(first / jnp.sqrt(second))
            RAW[c, u, x, zq] = jnp.concatenate(raws, axis=0).astype(BF)

            def send(d, _):
                az_copy(u, d).start()
                return 0

            lax.fori_loop(1, ZN, send, 0)
            pm_copy().start()

    def ax_copies(u):
        ref = RAW.at[c, u, x]
        return [
            remote(ref, ref, ax_s.at[u, d - 1], ax_r.at[u, d - 1], x=xat(d)) for d in (1, 2, 3)
        ]

    def az_stage(u):
        for q in range(ZQ):
            ref = RAW.at[c, u, x, q]
            pl.when(z != q * NC + u)(
                lambda: remote(ref, ref, az_s.at[1], az_r.at[u, q], z=zat(1)).wait_recv()
            )
        for copy in ax_copies(u):
            copy.start()

    def ad_copy(u):
        ref = RAW.at[c, u]
        return remote(ref, ref, ad_s.at[u], ad_r.at[u], core=other)

    def ax_stage(u):
        for d in (1, 2, 3):
            ref = RAW.at[c, u, xat(-d)]
            remote(ref, ref, ax_s.at[u, d - 1], ax_r.at[u, d - 1], x=xat(d)).wait_recv()
        ad_copy(u).start()

    def ad_stage(u):
        ref = RAW.at[other, u]
        remote(ref, ref, ad_s.at[u], ad_r.at[u], core=other).wait_recv()

    stages = ((y_stage, 0), (low_stage, 0), (rx_stage, 1), (rz_stage, 2), (az_stage, 3), (ax_stage, 4))
    late = {0: 2, 1: 3, 2: 4, 3: 5, 4: 6}
    for t in range(NC + 5):
        for stage, lag in stages:
            if 0 <= t - lag < NC:
                stage(t - lag)
        if t in late:
            master_steps[late[t]]()
            if late[t] == 6:
                whole[1].start()
    for u in range(NC):
        ad_stage(u)

    squares = jnp.zeros((8, 128), F32)
    for m in range(2):
        for u in range(NC):
            r = RAW[m, u].reshape(W, inner).astype(F32)
            r = (r * r).reshape(W // 8, 8, inner).sum(axis=0)
            for k in range(inner // 128):
                squares += r[:, k * 128 : (k + 1) * 128]
    SQ[y] = squares

    def sq_copy(d):
        return remote(SQ.at[y], SQ.at[y], sq_s.at[d - 1], sq_r.at[d - 1], tp=yat(d))

    for d in (1, 2, 3):
        sq_copy(d).start()
    for d in (1, 2, 3):
        ref = SQ.at[yat(-d)]
        remote(ref, ref, sq_s.at[d - 1], sq_r.at[d - 1], tp=yat(d)).wait_recv()
    total = jnp.sum(SQ[0] + SQ[1] + SQ[2] + SQ[3])
    scale = 0.25 * lax.rsqrt(
        jnp.full((1, inner), total, F32) / (2.0 * low_rank * inner * YN) + 1e-06
    )

    for k in range(2):
        src = BB.at[other] if k == 0 else MB.at[other]
        remote(src, src, d_s.at[k], d_r.at[k], core=other).wait_recv()

    TILE = 256

    def gate_out(t):
        rows = pl.ds(pl.multiple_of(t * TILE, TILE), TILE)
        return pltpu.make_async_copy(GO.at[rows], gcopy.at[rows], out_s.at[0, t])

    def out_out(t):
        rows = pl.ds(pl.multiple_of(t * 64, 64), 64)
        return pltpu.make_async_copy(OO.at[rows], ocopy.at[rows], out_s.at[1, t])

    raws = [RAW[m].reshape(low_rank, inner) for m in range(2)]

    def tile(t, _):
        zz = pl.ds(t * 2, 2)
        rows = pl.ds(pl.multiple_of(t * TILE, TILE), TILE)
        up = jnp.dot(BB[0, zz].reshape(TILE, low_rank), raws[0], preferred_element_type=F32)
        GO[rows] = (MB[0, zz].reshape(TILE, inner).astype(F32) - scale * up).astype(BF)
        gate_out(t).start()
        up = jnp.dot(BB[1, zz].reshape(TILE, low_rank), raws[1], preferred_element_type=F32)
        new = MB[1, zz].reshape(TILE, inner).astype(F32) - scale * up
        OO[:, rows] = new.T.astype(BF)
        return 0

    lax.fori_loop(0, 8, tile, 0)
    for t in range(8):
        out_out(t).start()

    pltpu.make_async_copy(gm, GM, ms.at[0]).wait()
    pltpu.make_async_copy(om, OM, ms.at[1]).wait()
    up = jnp.dot(BB[0, z, x, own_rows], raws[0], preferred_element_type=F32)
    GMO[...] = GM[...] - scale * up
    up = jnp.dot(BB[1, z, x, own_rows], raws[1], preferred_element_type=F32)
    OMO[...] = OM[...] - scale * up

    remote(PM, PM, pm_s, pm_r, core=other).wait_recv()

    def moments(mine, theirs):
        return [
            pltpu.make_async_copy(GMO, gm_out, ms.at[2]),
            pltpu.make_async_copy(OMO, om_out, ms.at[3]),
            pltpu.make_async_copy(NM.at[c, 0], mine[0], ms.at[4]),
            pltpu.make_async_copy(NM.at[c, 1], mine[1], ms.at[5]),
            pltpu.make_async_copy(PM.at[0], theirs[0], ms.at[6]),
            pltpu.make_async_copy(PM.at[1], theirs[1], ms.at[7]),
        ]

    def write(mine, theirs):
        for copy in moments(mine, theirs):
            copy.start()

    pl.when(c == 0)(lambda: write((gf_out, gs_out), (of_out, os_out)))
    pl.when(c == 1)(lambda: write((of_out, os_out), (gf_out, gs_out)))

    for k in range(6):
        ref = dsts[k](other)
        remote(gates[k], ref, ss.at[k], sr.at[k], core=other).wait_send()
    basis_finish()
    master_finish()
    for copy in whole:
        copy.wait_send()
    for u in range(NC):
        for copy in y_copies(u):
            copy.wait_send()
        _, _, a, b = y_relays(u)
        a.wait_send()
        b.wait_send()
        for copy in rx_copies(u) + ax_copies(u):
            copy.wait_send()
        for q in range(ZQ):
            pl.when(z != q * NC + u)(lambda: rz_copy(u, q).wait_send())
        ad_copy(u).wait_send()

    def sent(d, _):
        az_copy(0, d).wait_send()
        return 0

    lax.fori_loop(1, ZN, sent, 0)
    pm_copy().wait_send()
    for d in (1, 2, 3):
        sq_copy(d).wait_send()
    for t in range(8):
        gate_out(t).wait()
        out_out(t).wait()
    for copy in moments((gf_out, gs_out), (of_out, os_out)):
        copy.wait()


def on_device(
    block_input, gate_cotangent, gated_state, mixer_cotangent, gate_basis, out_basis,
    gate_master, out_master, gate_first, gate_second, out_first, out_second,
):
    low_rank = gate_basis.shape[1]
    inner = gate_first.shape[1]
    rows = gate_basis.shape[0]

    def by_owner(b):
        b = b.reshape(rows, ZQ, NC, XN, OWN)
        return b.transpose(0, 2, 3, 1, 4).reshape(rows, low_rank)

    out_t = out_master.T
    D = pltpu.SemaphoreType.DMA
    V = pltpu.VMEM
    full = rows * ZN * XN * 2
    W = low_rank // NC
    gather_sems = [
        D((NID,)), D((NID,)), D((2, NID)), D((2, NID)), D((2, NID)), D((2, NID)),
    ]
    outs = (
        jax.ShapeDtypeStruct((rows, inner), F32),
        jax.ShapeDtypeStruct((rows, inner), F32),
        jax.ShapeDtypeStruct((full, inner), BF),
        jax.ShapeDtypeStruct((inner, full), BF),
    ) + (jax.ShapeDtypeStruct(gate_first.shape, F32),) * 4
    res = pl.pallas_call(
        functools.partial(kernel, low_rank, inner),
        out_shape=outs,
        in_specs=[pl.BlockSpec(memory_space=pl.ANY)] * 14,
        out_specs=[pl.BlockSpec(memory_space=pl.ANY)] * 8,
        scratch_shapes=[
            V((2, 256, full), BF),
            V((2, 1024, inner), BF),
            V((2, ZN, XN, 32, low_rank), BF),
            V((2, ZN, XN, 32, inner), BF),
            V((YN, NC, W, 512), BF),
            V((NC, XN, ZQ, OWN, inner), BF),
            V((NC, 3, ZQ, OWN, inner), BF),
            V((NC, ZQ, OWN, inner), BF),
            V((ZN, OWN, inner), BF),
            V((2, NC, XN, ZQ, OWN, inner), BF),
            V((2, 2, 4, inner), F32),
            V((2, 2, 4, inner), F32),
            V((2, 4, inner), F32),
            V((YN, 8, 128), F32),
            V((full, inner), BF),
            V((inner, full), BF),
            V((rows, inner), F32),
            V((rows, inner), F32),
            V((rows, inner), F32),
            V((rows, inner), F32),
            D((6,)), D((6,)), D((6,)), D((8,)),
            *gather_sems,
            *gather_sems,
            D((2,)), D((2,)),
            D((2, NC)), D((2, NC)), D((2, NC)), D((2, NC)),
            D((NC, 3)), D((NC, 3)), D((NC, ZQ)), D((ZN,)),
            D((ZN,)), D((NC, ZQ)), D((NC, 3)), D((NC, 3)), D((NC,)), D((NC,)),
            D, D, D((3,)), D((3,)), D((2, 8)),
        ],
        compiler_params=pltpu.CompilerParams(
            collective_id=0, has_side_effects=True, vmem_limit_bytes=60 * 1024 * 1024
        ),
        name="moment_update",
    )(
        block_input, gate_cotangent, gated_state, mixer_cotangent,
        by_owner(gate_basis), by_owner(out_basis),
        gate_master.astype(BF), out_t.astype(BF), gate_master, out_t,
        gate_first, gate_second, out_first, out_second,
    )
    return (res[0], res[1].T, *res[2:])


def solution(mesh):
    finer = Mesh(mesh.devices.reshape(ZN, XN, 2, mesh.shape["tp"]), FS_TP)
    in_specs = (
        P(FS_TP, None), P(FSN, "tp"), P(FSN, "tp"), P(FS_TP, None), P(FSN, None), P(FSN, None),
        P(FSN, "tp"), P("tp", FSN), P(FSN, "tp"), P(FSN, "tp"), P(FSN, "tp"), P(FSN, "tp"),
    )
    out_specs = (
        P(FSN, "tp"), P("tp", FSN), P(None, "tp"), P("tp", None),
        P(FSN, "tp"), P(FSN, "tp"), P(FSN, "tp"), P(FSN, "tp"),
    )
    return jax.shard_map(
        on_device, mesh=finer, in_specs=in_specs, out_specs=out_specs, check_vma=False
    )
```

time: 494 us -> 127 us (0.26)
  blocking collectives: 234 us -> 0 us
  waiting for transfers between devices: 184 us -> 0 us
  Pallas kernels: 0 us -> 111 us
  starting transfers between devices: 22.6 us -> 0 us
  between operations: 15 us -> 0.68 us
  local copies, waits for them, and re-layouts: 23.8 us -> 12.8 us
  matrix products: 7.92 us -> 0 us
    all_to_all x9 -> x0, blocking collectives: 234 us -> none  [the longest x7 182 us: copy_for_each(): lax.all_to_all(jnp.broadcast_to(x[None], (peers, *x.shape)), axis, 0, 0,...]
    all_to_all x4 -> x0, waiting for transfers between devices: 152 us -> none  [copy_for_each(): lax.all_to_all(jnp.broadcast_to(x[None], (peers, *x.shape)), axis, 0, 0,...]
    pallas_call x0 -> x1, Pallas kernels: none -> 111 us  [on_device(): pl.pallas_call(functools.partial(kernel, low_rank, inner), out_shape=outs...]
    all_gather x1 -> x0, waiting for transfers between devices: 31.9 us -> none  [in_one_piece(): lax.all_gather(both, axis, axis=dim, tiled=True)]
    all_to_all x4 -> x0, starting transfers between devices: 22.5 us -> none  [copy_for_each(): lax.all_to_all(jnp.broadcast_to(x[None], (peers, *x.shape)), axis, 0, 0,...]
    broadcast_in_dim x11 -> x0, local copies, waits for them, and re-layouts: 9.13 us -> none  [copy_for_each(): jnp.broadcast_to(x[None], (peers, *x.shape))]
    dot_general x6 -> x0, matrix products: 7.92 us -> none  [the longest x1 2.25 us: on_device(): lax.dot_general(proj_cot, gated_state, contract, preferred_element_type=j...]
    unnamed x23 -> x20, local copies, waits for them, and re-layouts: 4.8 us -> 11.4 us
  transfers between devices with their start and end apart: 5 -> 0, of which waited for: 4 -> 0; matrix products, arithmetic and copies ran while one was open for 2% -> 0% of each run, Pallas kernels for 0% -> 0%
where the time goes in v1:
time: 127 us
  Pallas kernels  111 us (87%)
  local copies, waits for them, and re-layouts  12.8 us (10%)
  other arithmetic  2.73 us (2%)
    pallas_call x1, Pallas kernels, on_device(): pl.pallas_call(functools.partial(kernel, low_rank, inner), out_shape=outs...  111 us
    unnamed x20, local copies, waits for them, and re-layouts  11.4 us

profile of v1, /device:TPU:1, one launch (start us, length us, event | category | flops | bytes accessed | tf_op | source)
XLA Modules:
  0.0 126.9 jit_solution(7980193706511793905)
XLA Ops:
  0.6 1.4 %convert_element_type.6.gmb = bf16[16,512]{1,0:T(8,128)(2,1)} convert(f32[16,512]{1,0:T(8,128)} %gm.1) | non-fusion elementwise | flops 8192 | bytes 49152 | tf_op jit(solution)/shard_map/convert_element_type | solution.py:549
  2.0 1.4 %bitcast_convert_fusion.omb = bf16[16,512]{1,0:T(8,128)(2,1)} fusion(f32[512,16]{0,1:T(8,128)} %param.19), kind=kLoop, calls=%fused_computation | loop fusion | flops 8192 | bytes 49152 | tf_op jit(solution)/shard_map/convert_element_type | solution.py:549
  3.4 0.8 copy.22
  4.2 0.7 copy.26.gb
  4.9 0.8 copy.24
  5.8 0.7 copy.27.ob
  6.5 110.7 %moment_update.1 = (f32[16,512]{1,0:T(8,128)}, f32[16,512]{1,0:T(8,128)}, bf16[2048,512]{1,0:T(8,128)(2,1)}, bf16[512,2048]{1,0:T(8,128)(2,1)}, f32[4,512]{1,0:T...) custom-call(bf16[256,2048]{1,0:T(8,128)(2,1)} %bi.1, bf16[1024,512]{1,0:T(8,128)(2,1)} %gc.1, ...), custom_call_target="tpu_custom_call" | custom-call | tf_op jit(solution)/shard_map/moment_update/pallas_call | solution.py:507
  117.2 1.4 %copy.36 = f32[16,512]{1,0:T(8,128)} copy(f32[16,512]{1,0:T(8,128)} %get-tuple-element.32) | data formatting | bytes 65536
  118.6 1.4 %copy.37 = f32[512,16]{0,1:T(8,128)} copy(f32[512,16]{0,1:T(8,128)} %bitcast.16) | data formatting | bytes 65536
  120.0 0.0 copy-start
  120.0 3.2 %copy.38 = bf16[2048,512]{1,0:T(8,128)(2,1)} copy(bf16[2048,512]{1,0:T(8,128)(2,1)} %get-tuple-element.34) | data formatting | bytes 4194304
  123.2 0.0 copy-done
  123.2 0.0 copy-start.4
  123.2 0.0 copy-start.3
  123.2 0.0 copy-start.1
  123.2 1.3 %copy.39 = bf16[512,2048]{1,0:T(8,128)(2,1)} copy(bf16[512,2048]{1,0:T(8,128)(2,1)S(1)} %copy-done) | data formatting | bytes 4194304
  124.5 0.0 copy-done.4
  124.5 0.6 copy.40
  125.1 0.0 copy-done.3
  125.1 0.6 copy.41
  125.7 0.0 copy-done.2
  125.7 0.6 copy.42
  126.3 0.0 copy-done.1
  126.3 0.6 copy.43
  (3 shorter events, 0.1 us)
Async XLA Ops:
  120.0 3.2 %copy-start = (bf16[512,2048]{1,0:T(8,128)(2,1)S(1)}, bf16[512,2048]{1,0:T(8,128)(2,1)}, u32[]{:S(2)}) copy-start(bf16[512,2048]{1,0:T(8,128)(2,1)} %get-tuple-element.35) | copy-start | bytes 6291460
  123.2 1.3 %copy-start.4 = (f32[4,512]{1,0:T(4,128)S(1)}, f32[4,512]{1,0:T(4,128)}, u32[]{:S(2)}) copy-start(f32[4,512]{1,0:T(4,128)} %get-tuple-element.36) | copy-start | bytes 24580
  123.2 1.9 %copy-start.3 = (f32[4,512]{1,0:T(4,128)S(1)}, f32[4,512]{1,0:T(4,128)}, u32[]{:S(2)}) copy-start(f32[4,512]{1,0:T(4,128)} %get-tuple-element.37) | copy-start | bytes 24580
  123.2 2.5 %copy-start.2 = (f32[4,512]{1,0:T(4,128)S(1)}, f32[4,512]{1,0:T(4,128)}, u32[]{:S(2)}) copy-start(f32[4,512]{1,0:T(4,128)} %get-tuple-element.38) | copy-start | bytes 24580
  123.2 3.1 %copy-start.1 = (f32[4,512]{1,0:T(4,128)S(1)}, f32[4,512]{1,0:T(4,128)}, u32[]{:S(2)}) copy-start(f32[4,512]{1,0:T(4,128)} %get-tuple-element.39) | copy-start | bytes 24580

commit v2 on v1

v2 whole, which is shorter than its diff:
```python
import functools

import jax
import jax.numpy as jnp
from jax import lax
from jax.experimental import pallas as pl
from jax.experimental.pallas import tpu as pltpu
from jax.sharding import Mesh
from jax.sharding import PartitionSpec as P

MESH = pl.DeviceIdType.MESH
BF = jnp.bfloat16
F32 = jnp.float32
ZN, XN, YN = 16, 4, 4
FSN = ("z", "x", "core")
FS_TP = ("z", "x", "core", "tp")
NC = 4
ZQ = ZN // NC
OWN = 8
LIMIT1 = 32 * 1024 * 1024
LIMIT2 = 24 * 1024 * 1024
NID = ZN


def block_id(sign, dist):
    return 2 * dist - 1 if sign > 0 else 2 * dist


def remote(src, dst, send, recv, **to):
    return pltpu.make_async_remote_copy(
        src_ref=src, dst_ref=dst, send_sem=send, recv_sem=recv, device_id=to, device_id_type=MESH
    )


def kernel(
    low_rank, inner,
    bi, gc, gs, mc, gb, ob, gm, om, gf, gsec, of, osec,
    BB, MB, RAW, U, SQ, MO,
    X, C, BS, MS, PT, LB, XR, ZS, ZR, FS, NM,
    li, ss, sr,
    g_zs, g_zr, g_xs, g_xr, g_os, g_or,
    d_s, d_r,
    y_s, y_r, yo_s, yo_r,
    rx_s, rx_r, rz_s, rz_r,
    az_s, az_r, ax_s, ax_r, ad_s, ad_r,
    pm_s, pm_r, sq_s, sq_r,
):
    z, x, c, y = (lax.axis_index(a) for a in ("z", "x", "core", "tp"))
    other = 1 - c

    def zat(k):
        return lax.rem(z + k + ZN, ZN)

    def xat(k):
        return lax.rem(x + k + XN, XN)

    def yat(k):
        return lax.rem(y + k + YN, YN)

    dsts = (BS.at[c], X.at[c], C.at[c], MS.at[c], FS.at[0, c], FS.at[1, c])
    gates = (gb, bi, gc, gm, gf, gsec)
    outs = (ob, mc, gs, om, of, osec)

    def load(mine):
        for k in range(6):
            pltpu.make_async_copy(mine[k], dsts[k], li.at[k]).start()

    def ship(theirs):
        for k in range(6):
            remote(theirs[k], dsts[k], ss.at[k], sr.at[k], core=other).start()

    pl.when(c == 0)(lambda: load(gates))
    pl.when(c == 1)(lambda: load(outs))

    barrier = pltpu.get_barrier_semaphore()
    for k in (1, -1, 2, -2):
        pl.semaphore_signal(barrier, inc=1, device_id={"z": zat(k)}, device_id_type=MESH)
    for k in (1, -1):
        pl.semaphore_signal(barrier, inc=1, device_id={"x": xat(k)}, device_id_type=MESH)
        pl.semaphore_signal(barrier, inc=1, device_id={"tp": yat(k)}, device_id_type=MESH)
    pl.semaphore_signal(barrier, inc=1, device_id={"core": other}, device_id_type=MESH)

    at = lax.broadcasted_iota(jnp.int32, (low_rank, low_rank), 0)
    to = lax.broadcasted_iota(jnp.int32, (low_rank, low_rank), 1)
    source = ((to >> 3) & 3) * 128 + ((to >> 7) & 3) * 32 + ((to >> 5) & 3) * 8 + (to & 7)
    by_owner = jnp.where(at == source, 1.0, 0.0).astype(BF)

    pl.semaphore_wait(barrier, 9)

    pl.when(c == 0)(lambda: ship(outs))
    pl.when(c == 1)(lambda: ship(gates))

    def arrived(k):
        ref = dsts[k]
        pltpu.make_async_copy(gates[k], ref, li.at[k]).wait()
        remote(ref, ref, ss.at[k], sr.at[k], core=other).wait_recv()

    def gather(g, buf):
        zs, zr, xs, xr, os, orr = g_zs.at[g], g_zr.at[g], g_xs.at[g], g_xr.at[g], g_os.at[g], g_or.at[g]

        def got(ref, sem):
            remote(ref, ref, zs, sem, z=zat(1)).wait_recv()

        def zof(i):
            d = (i + 1) // 2
            return lax.rem(z + ZN + (1 - 2 * lax.rem(i, 2)) * d, ZN)

        def zsends(s):
            for sign, far in ((1, ZN // 2), (-1, ZN // 2 - 1)):
                src = buf.at[zat(-sign * 2 * s), x]
                for k in (2, 1):
                    if 2 * s + k <= far:
                        i = block_id(sign, 2 * s + k)
                        remote(src, src, zs, zr.at[(i - 1) // 2], z=zat(sign * k)).start()

        def zwait(k):
            got(buf.at[0:2, x] if k < 7 else buf.at[0, x], zr.at[k])

        def each(f, lo, hi):
            def body(i, _):
                f(i)
                return 0
            lax.fori_loop(lo, hi, body, 0)

        groups = ((0, 1), (1, 5), (5, 9), (9, 13), (13, 16))

        def forward(n):
            def one(i):
                ref = buf.at[zof(i), x]
                remote(ref, ref, xs, xr.at[n], x=xat(1)).start()
                remote(ref, ref, xs, xr.at[n], x=xat(-1)).start()
                if n == 4:
                    remote(ref, ref, os, orr, x=xat(2)).start()
            each(one, *groups[n])

        def relay(n):
            def one(i):
                zz = zof(i)
                a, b = buf.at[zz, xat(-1), pl.ds(0, 16)], buf.at[zz, xat(1), pl.ds(16, 16)]
                remote(a, a, os, orr, x=xat(1)).start()
                remote(b, b, os, orr, x=xat(-1)).start()
            lo, hi = groups[n]
            got(buf.at[0:2, 0] if n == 0 else buf.at[0:2], xr.at[n])
            each(one, lo, hi)

        def along_z(s):
            if s > 0:
                zwait(2 * s - 1)
            zsends(s)

        def along_x(n):
            if n > 0:
                zwait(2 * n - 2)
            if n == 4:
                zwait(7)
            forward(n)

        def opposite():
            got(buf.at[0:6, 0], xr.at[4])
            got(buf.at[0:4], orr)

        def finish():
            remote(buf.at[0:15, 0], buf.at[0:15, 0], zs, zr.at[0], z=zat(1)).wait_send()
            remote(buf.at[0:8], buf.at[0:8], xs, zr.at[0], z=zat(1)).wait_send()
            remote(buf.at[0:4], buf.at[0:4], os, zr.at[0], z=zat(1)).wait_send()

        return along_z, along_x, relay, opposite, finish

    Az, Ax, Ar, Ao, a_finish = gather(0, BB.at[c, 0])
    Bz, Bx, Br, Bo, b_finish = gather(1, BB.at[c, 1])
    Mz, Mx, Mr, Mo, m_finish = gather(2, MB.at[c])
    half = low_rank // 2

    arrived(0)
    ordered = jnp.dot(BS[...].reshape(32, low_rank), by_owner, preferred_element_type=F32).astype(BF)
    BB[c, 0, z, x] = ordered[:, :half]
    BB[c, 1, z, x] = ordered[:, half:]
    for s in range(4):
        Az(s)
        Ax(s)
        if s >= 2:
            Ar(s - 2)
        Bz(s)
        if s >= 1:
            Bx(s - 1)
    Ax(4)
    Ar(2)
    Bx(3)
    Br(0)
    arrived(3)
    MB[c, z, x] = MS[...].reshape(32, inner).astype(BF)
    Mz(0)
    Ar(3)
    Bx(4)
    Br(1)
    Br(2)
    Ao()
    arrived(1)

    W = low_rank // NC
    tokens = 512

    def y_copies(u):
        ref = PT.at[y, u]
        return [
            remote(ref, ref, y_s, y_r.at[0, u], tp=yat(1)),
            remote(ref, ref, y_s, y_r.at[1, u], tp=yat(-1)),
        ]

    def project(h):
        basis = BB[c, h].reshape(ZN * XN * 32, half)
        proj = jnp.dot(X[...].reshape(tokens, -1), basis, preferred_element_type=F32).T.astype(BF)
        for k in range(NC // 2):
            PT[y, h * (NC // 2) + k] = proj[k * W : (k + 1) * W]

    def send_projected(h):
        for k in range(NC // 2):
            for copy in y_copies(h * (NC // 2) + k):
                copy.start()

    def y_relays(u):
        left, right = PT.at[yat(-1), u], PT.at[yat(1), u]
        a, b = PT.at[yat(-1), u, pl.ds(0, W // 2)], PT.at[yat(1), u, pl.ds(W // 2, W // 2)]
        return (
            remote(left, left, y_s, y_r.at[0, u], tp=yat(1)),
            remote(right, right, y_s, y_r.at[1, u], tp=yat(-1)),
            remote(a, a, yo_s, yo_r.at[u], tp=yat(1)),
            remote(b, b, yo_s, yo_r.at[u], tp=yat(-1)),
        )

    def y_stage(u):
        l, r, a, b = y_relays(u)
        l.wait_recv()
        a.start()
        r.wait_recv()
        b.start()

    def rx_copies(u):
        return [
            remote(LB.at[u, xat(d)], XR.at[u, d - 1], rx_s, rx_r.at[u], x=xat(d))
            for d in (1, 2, 3)
        ]

    def low_stage(u):
        ref = PT.at[yat(2), u]
        remote(ref, ref, yo_s, yo_r.at[u], tp=yat(1)).wait_recv()

        def add(k, total):
            rows = pl.ds(pl.multiple_of(k * 256, 256), 256)
            for h in range(2):
                total += jnp.dot(
                    PT[k, u, :, h * 256 : (h + 1) * 256], C[h, rows], preferred_element_type=F32
                )
            return total

        total = lax.fori_loop(0, YN, add, jnp.zeros((W, inner), F32))
        LB[u] = total.reshape(XN, ZQ, OWN, inner).astype(BF)
        for copy in rx_copies(u):
            copy.start()

    def rz_copy(u, q):
        to = q * NC + u
        return remote(ZS.at[u, q], ZR.at[z], rz_s, rz_r, z=to)

    def rx_stage(u):
        total = LB[u, x].astype(F32)
        remote(XR.at[u], XR.at[u], rx_s, rx_r.at[u], x=xat(1)).wait_recv()
        for d in range(3):
            total += XR[u, d].astype(F32)
        ZS[u] = total.astype(BF)
        for q in range(ZQ):
            pl.when(z != q * NC + u)(lambda: rz_copy(u, q).start())

    zq = z // NC

    def az_copy(u, d):
        ref = RAW.at[c, u, x, zq]
        return remote(ref, ref, az_s, az_r.at[u], z=zat(d))

    def pm_copy():
        return remote(NM.at[other], MO.at[pl.ds(2 * c, 2)], pm_s, pm_r, core=other)

    def rz_stage(u):
        @pl.when(lax.rem(z, NC) == u)
        def _():
            def add(d, total):
                return total + ZR[zat(d)].astype(F32)

            remote(ZR.at[0:15], ZR.at[0:15], rz_s, rz_r, z=zat(1)).wait_recv()
            low = lax.fori_loop(1, ZN, add, ZS[u, zq].astype(F32))
            raws = []
            for h in range(2):
                part = low[4 * h : 4 * h + 4]
                first = 0.9 * FS[0, h] + 0.1 * part
                second = 0.95 * FS[1, h] + 0.05 * part * part
                NM[h, 0] = first
                NM[h, 1] = second
                raws.append(first / jnp.sqrt(second))
            RAW[c, u, x, zq] = jnp.concatenate(raws, axis=0).astype(BF)

            def send(d, _):
                az_copy(u, d).start()
                return 0

            lax.fori_loop(1, ZN, send, 0)
            pm_copy().start()
            MO[pl.ds(2 * c, 2)] = NM[c]

    def ax_copies(u):
        ref = RAW.at[c, u, x]
        return [
            remote(ref, ref, ax_s, ax_r.at[u], x=xat(d)) for d in (1, 2, 3)
        ]

    def az_stage(u):
        def landed(n):
            ref = RAW.at[c, u, x, pl.ds(0, n)]
            remote(ref, ref, az_s, az_r.at[u], z=zat(1)).wait_recv()

        pl.when(lax.rem(z, NC) == u)(lambda: landed(ZQ - 1))
        pl.when(lax.rem(z, NC) != u)(lambda: landed(ZQ))
        for copy in ax_copies(u):
            copy.start()

    def ad_copy(u):
        ref = RAW.at[c, u]
        return remote(ref, ref, ad_s, ad_r.at[u], core=other)

    def ax_stage(u):
        ref = RAW.at[c, u, pl.ds(0, 3)]
        remote(ref, ref, ax_s, ax_r.at[u], x=xat(1)).wait_recv()
        ad_copy(u).start()

    def ad_stage(u):
        ref = RAW.at[other, u]
        remote(ref, ref, ad_s, ad_r.at[u], core=other).wait_recv()

    project(0)
    send_projected(0)
    Br(3)
    Mz(1)
    whole = [
        remote(BB.at[c], BB.at[c], d_s.at[0], d_r.at[0], core=other),
        remote(MB.at[c], MB.at[c], d_s.at[1], d_r.at[1], core=other),
    ]
    Bo()
    project(1)
    y_stage(0)
    send_projected(1)
    whole[0].start()
    Mx(0)
    Mx(1)
    y_stage(1)
    Mz(2)
    Mx(2)
    for k in (2, 4, 5):
        arrived(k)
    low_stage(0)
    Mr(0)
    Mr(1)
    y_stage(2)
    Mz(3)
    Mx(3)
    y_stage(3)
    low_stage(1)
    rx_stage(0)
    Mr(2)
    low_stage(2)
    rx_stage(1)
    low_stage(3)
    Mx(4)
    rx_stage(2)
    rx_stage(3)
    Mr(3)
    for u in range(NC):
        rz_stage(u)
    az_stage(0)
    Mo()
    whole[1].start()
    for u in range(1, NC):
        az_stage(u)
    ax_stage(0)
    ax_stage(1)

    def begin(m):
        def some(t, _):
            zz, rows = pl.ds(t * 2, 2), pl.ds(pl.multiple_of(t * 256, 256), 256)
            U[m, rows] = jnp.dot(
                BB[m, 0, zz].reshape(256, half),
                RAW[m, 0 : NC // 2].reshape(half, inner),
                preferred_element_type=F32,
            )
            return 0

        lax.fori_loop(0, 8, some, 0)

    begin(c)
    ax_stage(2)
    ad_stage(0)
    ad_stage(1)
    remote(BB.at[other], BB.at[other], d_s.at[0], d_r.at[0], core=other).wait_recv()
    begin(other)

    def squares(m, u):
        r = RAW[m, u].reshape(W, inner).astype(F32)
        r = (r * r).reshape(W // 8, 8, inner).sum(axis=0)
        return sum(r[:, k * 128 : (k + 1) * 128] for k in range(inner // 128))

    total = jnp.zeros((8, 128), F32)
    for u in range(NC // 2):
        total += squares(0, u) + squares(1, u)
    ad_stage(2)
    total += squares(0, 2) + squares(1, 2)
    ax_stage(3)
    total += squares(c, 3)
    ad_stage(3)
    SQ[y] = total + squares(other, 3)

    def sq_copy(d):
        return remote(SQ.at[y], SQ.at[y], sq_s, sq_r, tp=yat(d))

    for d in (1, 2, 3):
        sq_copy(d).start()
    remote(SQ.at[0:3], SQ.at[0:3], sq_s, sq_r, tp=yat(1)).wait_recv()

    remote(MB.at[other], MB.at[other], d_s.at[1], d_r.at[1], core=other).wait_recv()
    remote(NM.at[c], NM.at[c], pm_s, pm_r, core=other).wait_recv()

    for k in range(6):
        remote(dsts[k], dsts[k], ss.at[k], sr.at[k], core=other).wait_send()
    a_finish()
    b_finish()
    m_finish()
    for copy in whole:
        copy.wait_send()
    for ref, sem in ((PT.at[0:2], y_s), (PT.at[0], yo_s), (XR, rx_s), (XR, ax_s), (LB, ad_s)):
        remote(ref, ref, sem, y_r.at[0, 0], tp=yat(1)).wait_send()
    fifteen = ZR.at[0:15]
    remote(fifteen, fifteen, rz_s, rz_r, z=zat(1)).wait_send()
    remote(fifteen, fifteen, az_s, rz_r, z=zat(1)).wait_send()
    pm_copy().wait_send()
    remote(SQ.at[0:3], SQ.at[0:3], sq_s, sq_r, tp=yat(1)).wait_send()


def finish(
    low_rank, inner,
    BB, MB, RAW, U, SQ, MO, gm, om,
    gm_out, om_out, gcopy, ocopy, gf_out, gs_out, of_out, os_out,
    GO, OO, out_s,
):
    z, x, c = (lax.axis_index(a) for a in ("z", "x", "core"))
    half = low_rank // 2
    own_rows = pl.ds(pl.multiple_of(c * 16, 16), 16)
    total = jnp.sum(SQ[0] + SQ[1] + SQ[2] + SQ[3])
    scale = 0.25 * lax.rsqrt(
        jnp.full((1, inner), total, F32) / (2.0 * low_rank * inner * YN) + 1e-06
    )
    TILE = 256

    def gate_out(t):
        rows = pl.ds(pl.multiple_of(t * TILE, TILE), TILE)
        return pltpu.make_async_copy(GO.at[rows], gcopy.at[rows], out_s.at[0, t])

    def out_out(t):
        rows = pl.ds(pl.multiple_of(t * TILE, TILE), TILE)
        return pltpu.make_async_copy(OO.at[:, rows], ocopy.at[:, rows], out_s.at[1, t])

    raws = [RAW[m, NC // 2 :].reshape(half, inner) for m in range(2)]

    def update(m, basis, rows):
        return scale * (U[m, rows] + jnp.dot(basis, raws[m], preferred_element_type=F32))

    def tile(t, _):
        zz = pl.ds(t * 2, 2)
        rows = pl.ds(pl.multiple_of(t * TILE, TILE), TILE)
        up = update(0, BB[0, 1, zz].reshape(TILE, half), rows)
        GO[rows] = (MB[0, zz].reshape(TILE, inner).astype(F32) - up).astype(BF)
        gate_out(t).start()
        up = update(1, BB[1, 1, zz].reshape(TILE, half), rows)
        OO[:, rows] = (MB[1, zz].reshape(TILE, inner).astype(F32) - up).T.astype(BF)
        out_out(t).start()
        return 0

    lax.fori_loop(0, 8, tile, 0)
    mine = pl.ds(pl.multiple_of((z * XN + x) * 32 + c * 16, 16), 16)
    gm_out[...] = gm[...] - update(0, BB[0, 1, z, x, own_rows], mine)
    om_out[...] = om[...] - update(1, BB[1, 1, z, x, own_rows], mine)
    for k, ref in enumerate((gf_out, gs_out, of_out, os_out)):
        ref[...] = MO[k]

    def done(t, _):
        gate_out(t).wait()
        out_out(t).wait()
        return 0

    lax.fori_loop(0, 8, done, 0)


def on_device(
    block_input, gate_cotangent, gated_state, mixer_cotangent, gate_basis, out_basis,
    gate_master, out_master, gate_first, gate_second, out_first, out_second,
):
    low_rank = gate_basis.shape[1]
    inner = gate_first.shape[1]
    rows = gate_basis.shape[0]

    out_t = out_master.T
    D = pltpu.SemaphoreType.DMA
    V = pltpu.VMEM
    full = rows * ZN * XN * 2
    W = low_rank // NC
    held = (
        jax.ShapeDtypeStruct((2, 2, ZN, XN, 32, low_rank // 2), BF),
        jax.ShapeDtypeStruct((2, ZN, XN, 32, inner), BF),
        jax.ShapeDtypeStruct((2, NC, XN, ZQ, OWN, inner), BF),
        jax.ShapeDtypeStruct((2, full, inner), F32),
        jax.ShapeDtypeStruct((YN, 8, 128), F32),
        jax.ShapeDtypeStruct((4, *gate_first.shape), F32),
    )
    vmem = pl.BlockSpec(memory_space=pltpu.VMEM)
    hbm = pl.BlockSpec(memory_space=pltpu.HBM)
    held = pl.pallas_call(
        functools.partial(kernel, low_rank, inner),
        out_shape=held,
        in_specs=[hbm] * 12,
        out_specs=[vmem] * 6,
        scratch_shapes=[
            V((2, 256, full), BF),
            V((2, 1024, inner), BF),
            V((2, rows, low_rank), BF),
            V((2, rows, inner), F32),
            V((YN, NC, W, 512), BF),
            V((NC, XN, ZQ, OWN, inner), BF),
            V((NC, 3, ZQ, OWN, inner), BF),
            V((NC, ZQ, OWN, inner), BF),
            V((ZN, OWN, inner), BF),
            V((2, 2, 4, inner), F32),
            V((2, 2, 4, inner), F32),
            D((6,)), D((6,)), D((6,)),
            D((3,)), D((3, NID // 2)), D((3,)), D((3, 5)), D((3,)), D((3,)),
            D((2,)), D((2,)),
            D, D((2, NC)), D, D((NC,)),
            D, D((NC,)), D, D,
            D, D((NC,)), D, D((NC,)), D, D((NC,)),
            D, D, D, D,
        ],
        compiler_params=pltpu.CompilerParams(
            collective_id=0, has_side_effects=True, vmem_limit_bytes=LIMIT1
        ),
        name="moment_update",
    )(
        *(pltpu.with_memory_space_constraint(a, pltpu.HBM) for a in (
            block_input, gate_cotangent, gated_state, mixer_cotangent, gate_basis, out_basis,
            gate_master, out_t, gate_first, gate_second, out_first, out_second,
        ))
    )
    outs = (
        jax.ShapeDtypeStruct((rows, inner), F32),
        jax.ShapeDtypeStruct((rows, inner), F32),
        jax.ShapeDtypeStruct((full, inner), BF),
        jax.ShapeDtypeStruct((inner, full), BF),
    ) + (jax.ShapeDtypeStruct(gate_first.shape, F32),) * 4
    res = pl.pallas_call(
        functools.partial(finish, low_rank, inner),
        out_shape=outs,
        in_specs=[vmem] * 8,
        out_specs=[vmem, vmem, hbm, hbm, vmem, vmem, vmem, vmem],
        scratch_shapes=[V((full, inner), BF), V((inner, full), BF), D((2, 8))],
        compiler_params=pltpu.CompilerParams(vmem_limit_bytes=LIMIT2),
        name="apply_step",
    )(*held, gate_master, out_t)
    return (res[0], res[1].T, *res[2:])


def solution(mesh):
    finer = Mesh(mesh.devices.reshape(ZN, XN, 2, mesh.shape["tp"]), FS_TP)
    in_specs = (
        P(FS_TP, None), P(FSN, "tp"), P(FSN, "tp"), P(FS_TP, None), P(FSN, None), P(FSN, None),
        P(FSN, "tp"), P("tp", FSN), P(FSN, "tp"), P(FSN, "tp"), P(FSN, "tp"), P(FSN, "tp"),
    )
    out_specs = (
        P(FSN, "tp"), P("tp", FSN), P(None, "tp"), P("tp", None),
        P(FSN, "tp"), P(FSN, "tp"), P(FSN, "tp"), P(FSN, "tp"),
    )
    return jax.shard_map(
        on_device, mesh=finer, in_specs=in_specs, out_specs=out_specs, check_vma=False
    )
```

time: 127 us -> 95.6 us (0.75)
  Pallas kernels: 111 us -> 94.8 us
  local copies, waits for them, and re-layouts: 12.8 us -> 0.01 us
  other arithmetic: 2.73 us -> 0 us
    pallas_call x1 -> x2, Pallas kernels: 111 us -> 94.8 us  [the longest x1 89.6 us: on_device(): pl.pallas_call(functools.partial(kernel, low_rank, inner), out_shape=held...]
    unnamed x20 -> x4, local copies, waits for them, and re-layouts: 11.4 us -> 0.01 us
    convert_element_type x2 -> x0, other arithmetic: 2.73 us -> none  [the longest x1 1.37 us: on_device(): gate_master.astype(BF)]
    reshape x2 -> x0, local copies, waits for them, and re-layouts: 1.38 us -> none  [by_owner(): return b.transpose(0, 2, 3, 1, 4).reshape(rows, low_rank)]
where the time goes in v2:
time: 95.6 us; the launch traced here: 95.5 us
  Pallas kernels  94.8 us (99%)
    pallas_call x1, Pallas kernels, on_device(): pl.pallas_call(functools.partial(kernel, low_rank, inner), out_shape=held...  89.6 us
    pallas_call x1, Pallas kernels, on_device(): pl.pallas_call(functools.partial(finish, low_rank, inner), out_shape=outs...  5.18 us

profile of v2, /device:TPU:1, one launch (start us, length us, event | category | flops | bytes accessed | tf_op | source)
XLA Modules:
  0.0 95.5 jit_solution(1799358399834012931)
XLA Ops:
  0.6 0.0 copy-start
  0.6 0.0 copy-start.1
  0.7 89.6 %moment_update.1 = (bf16[2,2,16,4,32,256]{5,4,3,2,1,0:T(8,128)(2,1)S(1)}, bf16[2,16,4,32,512]{4,3,2,1,0:T(8,128)(2,1)S(1)}, bf16[2,4,4,4,8,512]{5,4,3,2,1,0:T(8,...) custom-call(bf16[256,2048]{1,0:T(8,128)(2,1)} %bi.1, ...), custom_call_target="tpu_custom_call" | custom-call | tf_op jit(solution)/shard_map/moment_update/pallas_call | solution.py:522
  90.3 0.0 copy-done
  90.3 0.0 copy-done.1
  90.3 5.2 %apply_step.1 = (f32[16,512]{1,0:T(8,128)}, f32[16,512]{1,0:T(8,128)}, bf16[2048,512]{1,0:T(8,128)(2,1)}, bf16[512,2048]{1,0:T(8,128)(2,1)}, f32[4,512]{1,0:T(4,...) custom-call(bf16[2,2,16,4,32,256]{5,4,3,2,1,0:T(8,128)(2,1)S(1)} %get-tuple-element.22.BB, ...), custom_call_target="tpu_custom_call" | custom-call | tf_op jit(solution)/shard_map/apply_step/pallas_call | solution.py:563
Async XLA Ops:
  0.6 89.6 %copy-start = (f32[16,512]{1,0:T(8,128)S(1)}, f32[16,512]{1,0:T(8,128)}, u32[]{:S(2)}) copy-start(f32[16,512]{1,0:T(8,128)} %gm.3) | copy-start | bytes 98308
  0.6 89.6 %copy-start.1 = (f32[512,16]{0,1:T(8,128)S(1)}, f32[512,16]{0,1:T(8,128)}, u32[]{:S(2)}) copy-start(f32[512,16]{0,1:T(8,128)} %param.19) | copy-start | bytes 98308

commit v3 on v2

--- a/solution.py
+++ b/solution.py
@@ -17,8 +17,8 @@
 NC = 4
 ZQ = ZN // NC
 OWN = 8
-LIMIT1 = 32 * 1024 * 1024
-LIMIT2 = 24 * 1024 * 1024
+LIMIT1 = 30 * 1024 * 1024
+LIMIT2 = 8 * 1024 * 1024
 NID = ZN
 
 
@@ -35,8 +35,8 @@
 def kernel(
     low_rank, inner,
     bi, gc, gs, mc, gb, ob, gm, om, gf, gsec, of, osec,
-    BB, MB, RAW, U, SQ, MO,
-    X, C, BS, MS, PT, LB, XR, ZS, ZR, FS, NM,
+    MB, U, V, N, OR, SQ, MO,
+    BB, RAW, BT, RT, LP, X, C, BS, MS, PT, LB, XR, ZS, ZR, FS, NM,
     li, ss, sr,
     g_zs, g_zr, g_xs, g_xr, g_os, g_or,
     d_s, d_r,
@@ -185,12 +185,12 @@
             Bx(s - 1)
     Ax(4)
     Ar(2)
+    Ar(3)
     Bx(3)
     Br(0)
     arrived(3)
     MB[c, z, x] = MS[...].reshape(32, inner).astype(BF)
     Mz(0)
-    Ar(3)
     Bx(4)
     Br(1)
     Br(2)
@@ -213,10 +213,9 @@
         for k in range(NC // 2):
             PT[y, h * (NC // 2) + k] = proj[k * W : (k + 1) * W]
 
-    def send_projected(h):
-        for k in range(NC // 2):
-            for copy in y_copies(h * (NC // 2) + k):
-                copy.start()
+    def send_projected(u):
+        for copy in y_copies(u):
+            copy.start()
 
     def y_relays(u):
         left, right = PT.at[yat(-1), u], PT.at[yat(1), u]
@@ -238,22 +237,23 @@
     def rx_copies(u):
         return [
             remote(LB.at[u, xat(d)], XR.at[u, d - 1], rx_s, rx_r.at[u], x=xat(d))
-            for d in (1, 2, 3)
+            for d in (2, 3, 1)
         ]
+
+    def term(k, u):
+        rows = pl.ds(pl.multiple_of(k * 256, 256), 256)
+        return sum(
+            jnp.dot(PT[k, u, :, h * 256 : (h + 1) * 256], C[h, rows], preferred_element_type=F32)
+            for h in range(2)
+        )
+
+    def near_stage(u):
+        LP[...] = term(y, u) + term(yat(1), u) + term(yat(-1), u)
 
     def low_stage(u):
         ref = PT.at[yat(2), u]
         remote(ref, ref, yo_s, yo_r.at[u], tp=yat(1)).wait_recv()
-
-        def add(k, total):
-            rows = pl.ds(pl.multiple_of(k * 256, 256), 256)
-            for h in range(2):
-                total += jnp.dot(
-                    PT[k, u, :, h * 256 : (h + 1) * 256], C[h, rows], preferred_element_type=F32
-                )
-            return total
-
-        total = lax.fori_loop(0, YN, add, jnp.zeros((W, inner), F32))
+        total = LP[...] + term(yat(2), u)
         LB[u] = total.reshape(XN, ZQ, OWN, inner).astype(BF)
         for copy in rx_copies(u):
             copy.start()
@@ -298,18 +298,18 @@
                 raws.append(first / jnp.sqrt(second))
             RAW[c, u, x, zq] = jnp.concatenate(raws, axis=0).astype(BF)
 
-            def send(d, _):
-                az_copy(u, d).start()
+            def send(k, _):
+                az_copy(u, ZN // 2 + (k + 1) // 2 * (1 - 2 * lax.rem(k, 2))).start()
                 return 0
 
-            lax.fori_loop(1, ZN, send, 0)
+            lax.fori_loop(0, ZN - 1, send, 0)
             pm_copy().start()
             MO[pl.ds(2 * c, 2)] = NM[c]
 
     def ax_copies(u):
         ref = RAW.at[c, u, x]
         return [
-            remote(ref, ref, ax_s, ax_r.at[u], x=xat(d)) for d in (1, 2, 3)
+            remote(ref, ref, ax_s, ax_r.at[u], x=xat(d)) for d in (2, 3, 1)
         ]
 
     def az_stage(u):
@@ -337,69 +337,108 @@
 
     project(0)
     send_projected(0)
+    send_projected(1)
     Br(3)
     Mz(1)
+    Mx(0)
+    Mx(1)
     whole = [
         remote(BB.at[c], BB.at[c], d_s.at[0], d_r.at[0], core=other),
         remote(MB.at[c], MB.at[c], d_s.at[1], d_r.at[1], core=other),
     ]
     Bo()
     project(1)
-    y_stage(0)
-    send_projected(1)
-    whole[0].start()
-    Mx(0)
-    Mx(1)
-    y_stage(1)
     Mz(2)
     Mx(2)
+    y_stage(0)
+    send_projected(2)
+    whole[0].start()
+    Mr(0)
+    y_stage(1)
+    send_projected(3)
+    Mr(1)
+    Mz(3)
+    Mx(3)
     for k in (2, 4, 5):
         arrived(k)
+    near_stage(0)
     low_stage(0)
-    Mr(0)
-    Mr(1)
+    near_stage(1)
     y_stage(2)
-    Mz(3)
-    Mx(3)
+    Mr(2)
+    low_stage(1)
+    near_stage(2)
     y_stage(3)
-    low_stage(1)
     rx_stage(0)
-    Mr(2)
     low_stage(2)
+    near_stage(3)
+    Mx(4)
     rx_stage(1)
     low_stage(3)
-    Mx(4)
+    Mr(3)
     rx_stage(2)
     rx_stage(3)
-    Mr(3)
     for u in range(NC):
         rz_stage(u)
-    az_stage(0)
     Mo()
     whole[1].start()
-    for u in range(1, NC):
-        az_stage(u)
+    remote(BB.at[other], BB.at[other], d_s.at[0], d_r.at[0], core=other).wait_recv()
+
+    def turn_basis(t, _):
+        rows = pl.ds(pl.multiple_of(t * 256, 256), 256)
+        for h in range(2):
+            BT[h, :, rows] = BB[1, h, pl.ds(t * 2, 2)].reshape(256, half).T
+        return 0
+
+    lax.fori_loop(0, 8, turn_basis, 0)
+    az_stage(0)
+    az_stage(1)
+    landed = remote(MB.at[other], MB.at[other], d_s.at[1], d_r.at[1], core=other)
+    pl.when(c == 0)(landed.wait_recv)
+
+    def turn(t, _):
+        rows = pl.ds(pl.multiple_of(t * 256, 256), 256)
+        N[:, rows] = MB[1, pl.ds(t * 2, 2)].reshape(256, inner).T
+        return 0
+
+    lax.fori_loop(0, 8, turn, 0)
+    az_stage(2)
     ax_stage(0)
+    az_stage(3)
     ax_stage(1)
 
-    def begin(m):
+    def raw_half(m, h):
+        return RAW[m, h * (NC // 2) : (h + 1) * (NC // 2)].reshape(half, inner)
+
+    def gate_half(h):
         def some(t, _):
-            zz, rows = pl.ds(t * 2, 2), pl.ds(pl.multiple_of(t * 256, 256), 256)
-            U[m, rows] = jnp.dot(
-                BB[m, 0, zz].reshape(256, half),
-                RAW[m, 0 : NC // 2].reshape(half, inner),
-                preferred_element_type=F32,
+            zz, rows = pl.ds(t * 8, 8), pl.ds(pl.multiple_of(t * 1024, 1024), 1024)
+            part = jnp.dot(
+                BB[0, h, zz].reshape(1024, half), raw_half(0, h), preferred_element_type=F32
             )
+            U[rows] = part if h == 0 else U[rows] + part
             return 0
 
-        lax.fori_loop(0, 8, some, 0)
-
-    begin(c)
+        lax.fori_loop(0, 2, some, 0)
+
+    def out_half(h):
+        RT[...] = raw_half(1, h).T
+
+        def some(t, _):
+            rows = pl.ds(pl.multiple_of(t * 1024, 1024), 1024)
+            part = jnp.dot(RT[...], BT[h, :, rows], preferred_element_type=F32)
+            V[:, rows] = part if h == 0 else V[:, rows] + part
+            return 0
+
+        lax.fori_loop(0, 2, some, 0)
+
+    pl.when(c == 0)(lambda: gate_half(0))
+    pl.when(c == 1)(lambda: out_half(0))
     ax_stage(2)
     ad_stage(0)
     ad_stage(1)
-    remote(BB.at[other], BB.at[other], d_s.at[0], d_r.at[0], core=other).wait_recv()
-    begin(other)
+    pl.when(c == 0)(lambda: out_half(0))
+    pl.when(c == 1)(lambda: gate_half(0))
 
     def squares(m, u):
         r = RAW[m, u].reshape(W, inner).astype(F32)
@@ -421,9 +460,17 @@
 
     for d in (1, 2, 3):
         sq_copy(d).start()
+
+    gate_half(1)
+    out_half(1)
+    own_rows = pl.ds(pl.multiple_of(c * 16, 16), 16)
+    OR[...] = sum(
+        jnp.dot(BB[1, h, z, x, own_rows], raw_half(1, h), preferred_element_type=F32)
+        for h in range(2)
+    )
     remote(SQ.at[0:3], SQ.at[0:3], sq_s, sq_r, tp=yat(1)).wait_recv()
 
-    remote(MB.at[other], MB.at[other], d_s.at[1], d_r.at[1], core=other).wait_recv()
+    pl.when(c == 1)(landed.wait_recv)
     remote(NM.at[c], NM.at[c], pm_s, pm_r, core=other).wait_recv()
 
     for k in range(6):
@@ -444,17 +491,23 @@
 
 def finish(
     low_rank, inner,
-    BB, MB, RAW, U, SQ, MO, gm, om,
+    MB, U, V, N, OR, SQ, MO, gm, om,
     gm_out, om_out, gcopy, ocopy, gf_out, gs_out, of_out, os_out,
-    GO, OO, out_s,
+    GO, OO, GMO, OMO, out_s, few_s,
 ):
     z, x, c = (lax.axis_index(a) for a in ("z", "x", "core"))
-    half = low_rank // 2
-    own_rows = pl.ds(pl.multiple_of(c * 16, 16), 16)
     total = jnp.sum(SQ[0] + SQ[1] + SQ[2] + SQ[3])
-    scale = 0.25 * lax.rsqrt(
-        jnp.full((1, inner), total, F32) / (2.0 * low_rank * inner * YN) + 1e-06
-    )
+    full = GO.shape[0]
+    few = [
+        pltpu.make_async_copy(MO.at[k], ref, few_s.at[k])
+        for k, ref in enumerate((gf_out, gs_out, of_out, os_out))
+    ]
+    for copy in few:
+        copy.start()
+    scale_t = 0.25 * lax.rsqrt(
+        jnp.full((1, full), total, F32) / (2.0 * low_rank * inner * YN) + 1e-06
+    )
+    scale = scale_t[:, :inner]
     TILE = 256
 
     def gate_out(t):
@@ -462,38 +515,38 @@
         return pltpu.make_async_copy(GO.at[rows], gcopy.at[rows], out_s.at[0, t])
 
     def out_out(t):
-        rows = pl.ds(pl.multiple_of(t * TILE, TILE), TILE)
-        return pltpu.make_async_copy(OO.at[:, rows], ocopy.at[:, rows], out_s.at[1, t])
-
-    raws = [RAW[m, NC // 2 :].reshape(half, inner) for m in range(2)]
-
-    def update(m, basis, rows):
-        return scale * (U[m, rows] + jnp.dot(basis, raws[m], preferred_element_type=F32))
+        rows = pl.ds(pl.multiple_of(t * 64, 64), 64)
+        return pltpu.make_async_copy(OO.at[rows], ocopy.at[rows], out_s.at[1, t])
 
     def tile(t, _):
         zz = pl.ds(t * 2, 2)
         rows = pl.ds(pl.multiple_of(t * TILE, TILE), TILE)
-        up = update(0, BB[0, 1, zz].reshape(TILE, half), rows)
-        GO[rows] = (MB[0, zz].reshape(TILE, inner).astype(F32) - up).astype(BF)
+        GO[rows] = (MB[0, zz].reshape(TILE, inner).astype(F32) - scale * U[rows]).astype(BF)
         gate_out(t).start()
-        up = update(1, BB[1, 1, zz].reshape(TILE, half), rows)
-        OO[:, rows] = (MB[1, zz].reshape(TILE, inner).astype(F32) - up).T.astype(BF)
+        rows = pl.ds(pl.multiple_of(t * 64, 64), 64)
+        OO[rows] = (N[rows].astype(F32) - scale_t * V[rows]).astype(BF)
         out_out(t).start()
         return 0
 
+    mine = pl.ds(pl.multiple_of((z * XN + x) * 32 + c * 16, 16), 16)
+    GMO[...] = gm[...] - scale * U[mine]
+    OMO[...] = om[...] - scale * OR[...]
+    few += [
+        pltpu.make_async_copy(GMO, gm_out, few_s.at[4]),
+        pltpu.make_async_copy(OMO, om_out, few_s.at[5]),
+    ]
+    for copy in few[4:]:
+        copy.start()
     lax.fori_loop(0, 8, tile, 0)
     mine = pl.ds(pl.multiple_of((z * XN + x) * 32 + c * 16, 16), 16)
-    gm_out[...] = gm[...] - update(0, BB[0, 1, z, x, own_rows], mine)
-    om_out[...] = om[...] - update(1, BB[1, 1, z, x, own_rows], mine)
-    for k, ref in enumerate((gf_out, gs_out, of_out, os_out)):
-        ref[...] = MO[k]
-
     def done(t, _):
         gate_out(t).wait()
         out_out(t).wait()
         return 0
 
     lax.fori_loop(0, 8, done, 0)
+    for copy in few:
+        copy.wait()
 
 
 def on_device(
@@ -506,14 +559,15 @@
 
     out_t = out_master.T
     D = pltpu.SemaphoreType.DMA
-    V = pltpu.VMEM
+    vm = pltpu.VMEM
     full = rows * ZN * XN * 2
     W = low_rank // NC
     held = (
-        jax.ShapeDtypeStruct((2, 2, ZN, XN, 32, low_rank // 2), BF),
         jax.ShapeDtypeStruct((2, ZN, XN, 32, inner), BF),
-        jax.ShapeDtypeStruct((2, NC, XN, ZQ, OWN, inner), BF),
-        jax.ShapeDtypeStruct((2, full, inner), F32),
+        jax.ShapeDtypeStruct((full, inner), F32),
+        jax.ShapeDtypeStruct((inner, full), F32),
+        jax.ShapeDtypeStruct((inner, full), BF),
+        jax.ShapeDtypeStruct((rows, inner), F32),
         jax.ShapeDtypeStruct((YN, 8, 128), F32),
         jax.ShapeDtypeStruct((4, *gate_first.shape), F32),
     )
@@ -523,19 +577,24 @@
         functools.partial(kernel, low_rank, inner),
         out_shape=held,
         in_specs=[hbm] * 12,
-        out_specs=[vmem] * 6,
+        out_specs=[vmem] * 7,
         scratch_shapes=[
-            V((2, 256, full), BF),
-            V((2, 1024, inner), BF),
-            V((2, rows, low_rank), BF),
-            V((2, rows, inner), F32),
-            V((YN, NC, W, 512), BF),
-            V((NC, XN, ZQ, OWN, inner), BF),
-            V((NC, 3, ZQ, OWN, inner), BF),
-            V((NC, ZQ, OWN, inner), BF),
-            V((ZN, OWN, inner), BF),
-            V((2, 2, 4, inner), F32),
-            V((2, 2, 4, inner), F32),
+            vm((2, 2, ZN, XN, 32, low_rank // 2), BF),
+            vm((2, NC, XN, ZQ, OWN, inner), BF),
+            vm((2, low_rank // 2, full), BF),
+            vm((inner, low_rank // 2), BF),
+            vm((W, inner), F32),
+            vm((2, 256, full), BF),
+            vm((2, 1024, inner), BF),
+            vm((2, rows, low_rank), BF),
+            vm((2, rows, inner), F32),
+            vm((YN, NC, W, 512), BF),
+            vm((NC, XN, ZQ, OWN, inner), BF),
+            vm((NC, 3, ZQ, OWN, inner), BF),
+            vm((NC, ZQ, OWN, inner), BF),
+            vm((ZN, OWN, inner), BF),
+            vm((2, 2, 4, inner), F32),
+            vm((2, 2, 4, inner), F32),
             D((6,)), D((6,)), D((6,)),
             D((3,)), D((3, NID // 2)), D((3,)), D((3, 5)), D((3,)), D((3,)),
             D((2,)), D((2,)),
@@ -563,9 +622,12 @@
     res = pl.pallas_call(
         functools.partial(finish, low_rank, inner),
         out_shape=outs,
-        in_specs=[vmem] * 8,
-        out_specs=[vmem, vmem, hbm, hbm, vmem, vmem, vmem, vmem],
-        scratch_shapes=[V((full, inner), BF), V((inner, full), BF), D((2, 8))],
+        in_specs=[vmem] * 9,
+        out_specs=[hbm] * 8,
+        scratch_shapes=[
+            vm((full, inner), BF), vm((inner, full), BF), vm((rows, inner), F32), vm((rows, inner), F32),
+            D((2, 8)), D((6,)),
+        ],
         compiler_params=pltpu.CompilerParams(vmem_limit_bytes=LIMIT2),
         name="apply_step",
     )(*held, gate_master, out_t)

time: 95.6 us -> 89.9 us (0.940)
  Pallas kernels: 94.8 us -> 89 us
    pallas_call x1, Pallas kernels: 89.6 us -> 86.6 us  [on_device(): pl.pallas_call(functools.partial(kernel, low_rank, inner), out_shape=held...]
    pallas_call x1, Pallas kernels: 5.18 us -> 2.4 us  [on_device(): pl.pallas_call(functools.partial(finish, low_rank, inner), out_shape=outs...]
where the time goes in v3:
time: 89.9 us; the launch traced here: 89.7 us
  Pallas kernels  89 us (99%)
    pallas_call x1, Pallas kernels, on_device(): pl.pallas_call(functools.partial(kernel, low_rank, inner), out_shape=held...  86.6 us
    pallas_call x1, Pallas kernels, on_device(): pl.pallas_call(functools.partial(finish, low_rank, inner), out_shape=outs...  2.4 us

profile of v3, /device:TPU:1, one launch (start us, length us, event | category | flops | bytes accessed | tf_op | source)
XLA Modules:
  0.0 89.7 jit_solution(11476436310560145444)
XLA Ops:
  0.6 0.0 copy-start
  0.6 0.0 copy-start.1
  0.7 86.6 %moment_update.1 = (bf16[2,16,4,32,512]{4,3,2,1,0:T(8,128)(2,1)S(1)}, f32[2048,512]{1,0:T(8,128)S(1)}, f32[512,2048]{1,0:T(8,128)S(1)}, bf16[512,2048]{1,0:T(8,1...) custom-call(bf16[256,2048]{1,0:T(8,128)(2,1)} %bi.1, ...), custom_call_target="tpu_custom_call" | custom-call | tf_op jit(solution)/shard_map/moment_update/pallas_call | solution.py:576
  87.3 0.0 copy-done
  87.3 0.0 copy-done.1
  87.3 2.4 %apply_step.1 = (f32[16,512]{1,0:T(8,128)}, f32[16,512]{1,0:T(8,128)}, bf16[2048,512]{1,0:T(8,128)(2,1)}, bf16[512,2048]{1,0:T(8,128)(2,1)}, f32[4,512]{1,0:T(4,...) custom-call(bf16[2,16,4,32,512]{4,3,2,1,0:T(8,128)(2,1)S(1)} %get-tuple-element.23.MB, ...), custom_call_target="tpu_custom_call" | custom-call | tf_op jit(solution)/shard_map/apply_step/pallas_call | solution.py:622
Async XLA Ops:
  0.6 86.7 %copy-start = (f32[16,512]{1,0:T(8,128)S(1)}, f32[16,512]{1,0:T(8,128)}, u32[]{:S(2)}) copy-start(f32[16,512]{1,0:T(8,128)} %gm.3) | copy-start | bytes 98308
  0.6 86.7 %copy-start.1 = (f32[512,16]{0,1:T(8,128)S(1)}, f32[512,16]{0,1:T(8,128)}, u32[]{:S(2)}) copy-start(f32[512,16]{0,1:T(8,128)} %param.19) | copy-start | bytes 98308

commit v4 on v3

--- a/solution.py
+++ b/solution.py
@@ -353,9 +353,9 @@
     y_stage(0)
     send_projected(2)
     whole[0].start()
+    send_projected(3)
     Mr(0)
     y_stage(1)
-    send_projected(3)
     Mr(1)
     Mz(3)
     Mx(3)
@@ -372,9 +372,9 @@
     rx_stage(0)
     low_stage(2)
     near_stage(3)
+    low_stage(3)
     Mx(4)
     rx_stage(1)
-    low_stage(3)
     Mr(3)
     rx_stage(2)
     rx_stage(3)

time: 89.9 us -> 88.2 us (0.981)
  Pallas kernels: 89 us -> 87.3 us
    pallas_call x1, Pallas kernels: 86.6 us -> 84.9 us  [on_device(): pl.pallas_call(functools.partial(kernel, low_rank, inner), out_shape=held...]
where the time goes in v4:
time: 88.2 us; the launch traced here: 88 us
  Pallas kernels  87.3 us (99%)
    pallas_call x1, Pallas kernels, on_device(): pl.pallas_call(functools.partial(kernel, low_rank, inner), out_shape=held...  84.9 us
    pallas_call x1, Pallas kernels, on_device(): pl.pallas_call(functools.partial(finish, low_rank, inner), out_shape=outs...  2.4 us

profile of v4, /device:TPU:1, one launch (start us, length us, event | category | flops | bytes accessed | tf_op | source)
XLA Modules:
  0.0 88.0 jit_solution(4593248542865242456)
XLA Ops:
  0.6 0.0 copy-start
  0.6 0.0 copy-start.1
  0.7 84.9 %moment_update.1 = (bf16[2,16,4,32,512]{4,3,2,1,0:T(8,128)(2,1)S(1)}, f32[2048,512]{1,0:T(8,128)S(1)}, f32[512,2048]{1,0:T(8,128)S(1)}, bf16[512,2048]{1,0:T(8,1...) custom-call(bf16[256,2048]{1,0:T(8,128)(2,1)} %bi.1, ...), custom_call_target="tpu_custom_call" | custom-call | tf_op jit(solution)/shard_map/moment_update/pallas_call | solution.py:576
  85.6 0.0 copy-done
  85.6 0.0 copy-done.1
  85.6 2.4 %apply_step.1 = (f32[16,512]{1,0:T(8,128)}, f32[16,512]{1,0:T(8,128)}, bf16[2048,512]{1,0:T(8,128)(2,1)}, bf16[512,2048]{1,0:T(8,128)(2,1)}, f32[4,512]{1,0:T(4,...) custom-call(bf16[2,16,4,32,512]{4,3,2,1,0:T(8,128)(2,1)S(1)} %get-tuple-element.23.MB, ...), custom_call_target="tpu_custom_call" | custom-call | tf_op jit(solution)/shard_map/apply_step/pallas_call | solution.py:622
Async XLA Ops:
  0.6 84.9 %copy-start = (f32[16,512]{1,0:T(8,128)S(1)}, f32[16,512]{1,0:T(8,128)}, u32[]{:S(2)}) copy-start(f32[16,512]{1,0:T(8,128)} %gm.3) | copy-start | bytes 98308
  0.6 84.9 %copy-start.1 = (f32[512,16]{0,1:T(8,128)S(1)}, f32[512,16]{0,1:T(8,128)}, u32[]{:S(2)}) copy-start(f32[512,16]{0,1:T(8,128)} %param.19) | copy-start | bytes 98308
